TPU v7x, 32 devices: a whole 2x2x4 slice. The times are simulated.
32 devices in a mesh: sp: 4 (over z), tp: 4 (over y, x), dp: 2 (over core).
Axes of the slice: x: 2, y: 2, z: 4, core: 2. Of those that a mesh axis runs over, the one named last changes fastest.
Arguments:
- latent: bfloat16 [2048, 4, 2048], P(('sp', 'tp'), 'dp'), may hold values from -6 to 6
- context: bfloat16 [1024, 4, 2048], P('sp', 'dp'), may hold values from -6 to 6
- condition: bfloat16 [4, 2048], P('dp', 'sp'), may hold values from -6 to 6
- ctx_condition: bfloat16 [2048], P('sp'), may hold values from -6 to 6
- norm_gain: float32 [2048], replicated, may hold values from 0.1 to 1.9
- w_shift: bfloat16 [2048, 2048], P('sp', 'tp'), may hold values from -0.1875 to 0.1875
- w_scale: bfloat16 [2048, 2048], P('sp', 'tp'), may hold values from -0.1875 to 0.1875
- w_gate: bfloat16 [2048, 2048], P('sp', 'tp'), may hold values from -0.1875 to 0.1875
- w_query: bfloat16 [2048, 2048], P(None, 'tp'), may hold values from -0.125 to 0.125
- w_key: bfloat16 [2048, 512], P(None, 'tp'), may hold values from -6 to 6
- w_value: bfloat16 [2048, 512], P(None, 'tp'), may hold values from -0.125 to 0.125
- w_out: bfloat16 [2048, 2048], P('tp'), may hold values from -1 to 1
- sink: float32 [16], P('tp'), may hold values from 5 to 9
Outputs:
- mixed: bfloat16 [2048, 4, 2048], P(('sp', 'tp'), 'dp')
All inputs are finite; a program needn't handle non-finite values.
Results may differ from a plain program's by a relative error of at most 0.015.
The roundings to bfloat16 on the way count: a program that leaves them out, or rounds other values in their place, can miss the bound.
Values may be sent and summed in bfloat16 or wider, within the bound.
A program may use at most 128 MiB of HBM per device.

v0:
```python
import functools
import math

import jax
import jax.numpy as jnp
from jax import lax
from jax.experimental import pallas as pl
from jax.experimental.pallas import tpu as pltpu
from jax.sharding import PartitionSpec as P

HEAD_DIM = 128
WINDOW = 128
GRID_W = 64
EPSILON = 1e-06
NEGATIVE = -1e30
MESH = pl.DeviceIdType.MESH
F32 = jnp.float32
BF16 = jnp.bfloat16
LOG2E = math.log2(math.e)
CHUNK = 16
SENDS = ((3, 0), (3, 1), (1, 0), (2, 1), (2, 0), (1, 1), (0, 0), (0, 1))
TARGETS = (1, 2, 1, 2, 2, 1)


def kernel(
    n_sp,
    lat_hbm,
    ctx_hbm,
    cond_ref,
    cctx_ref,
    gain_ref,
    wsh_hbm,
    wsc_hbm,
    wga_hbm,
    wq_hbm,
    wk_hbm,
    wv_hbm,
    wo_hbm,
    sink_ref,
    row_cos,
    row_sin,
    col_cos,
    col_sin,
    out_ref,
    lat_all,
    ctx_v,
    wmod,
    wqkv,
    wo,
    act_s,
    mod_p,
    mod_all,
    mod_a,
    mod_b,
    mod_g,
    hbuf,
    qbuf,
    kvbuf,
    ckv,
    abuf,
    cos_ref,
    sin_ref,
    psend,
    rs,

    loc_sem,
    modp_s,
    modp_r,
    moda_s,
    moda_r,
    lat_s,
    lat_r,
    early_s,
    early_r,
    ctx_s,
    ctx_r,
    halo_s,
    halo_r,
    rs_s,
    rs_r,
):
    samples, rows, width = lat_hbm.shape
    n_tp = mod_all.shape[0]
    wid = wmod.shape[2]
    qw = wq_hbm.shape[1]
    kw = wk_hbm.shape[1]
    heads = qw // HEAD_DIM
    lc = ctx_hbm.shape[1]
    block = rows * n_tp
    sp = lax.axis_index("sp")
    tp = lax.axis_index("tp")
    tx, ty = tp % 2, tp // 2
    peer = {1: 2 * ty + 1 - tx, 2: 2 * (1 - ty) + tx, 3: 3 - tp}

    def sp_peer(o):
        return lax.rem(sp + o, n_sp)

    loads = [
        pltpu.make_async_copy(wsh_hbm, wmod.at[0], loc_sem.at[0]),
        pltpu.make_async_copy(wsc_hbm, wmod.at[1], loc_sem.at[1]),
        pltpu.make_async_copy(wga_hbm, wmod.at[2], loc_sem.at[2]),
        pltpu.make_async_copy(ctx_hbm, ctx_v, loc_sem.at[3]),
        pltpu.make_async_copy(wk_hbm, wqkv.at[:, pl.ds(qw, kw)], loc_sem.at[4]),
        pltpu.make_async_copy(wv_hbm, wqkv.at[:, pl.ds(qw + kw, kw)], loc_sem.at[5]),
        pltpu.make_async_copy(lat_hbm, lat_all.at[0], loc_sem.at[6]),
        pltpu.make_async_copy(wq_hbm, wqkv.at[:, pl.ds(0, qw)], loc_sem.at[7]),
        pltpu.make_async_copy(wo_hbm, wo, loc_sem.at[8]),
    ]
    for load in loads:
        load.start()

    barrier = pltpu.get_barrier_semaphore()
    for o in range(1, n_sp):
        pl.semaphore_signal(barrier, inc=1, device_id={"sp": sp_peer(o)}, device_id_type=MESH)
    for k in (1, 2, 3):
        pl.semaphore_signal(barrier, inc=1, device_id={"tp": peer[k]}, device_id_type=MESH)
    pl.semaphore_wait(barrier, n_sp - 1 + n_tp - 1)

    def remote(src, dst, ssem, rsem, dev):
        return pltpu.make_async_remote_copy(
            src_ref=src, dst_ref=dst, send_sem=ssem, recv_sem=rsem, device_id=dev, device_id_type=MESH
        )

    act_s[...] = jnp.zeros_like(act_s)
    cv = cond_ref[...].astype(F32)
    act_s[0:samples, :] = cv / (1.0 + jnp.exp(-cv))
    cc = cctx_ref[...].astype(F32).reshape(1, -1)
    act_s[samples : samples + 1, :] = cc / (1.0 + jnp.exp(-cc))
    both = act_s[...].astype(BF16)
    for m in range(3):
        loads[m].wait()
        mod_p[0, :, m * wid : (m + 1) * wid] = jnp.dot(both, wmod[m], preferred_element_type=F32)
    mod_copies = [
        remote(mod_p.at[0], mod_p.at[o], modp_s.at[o], modp_r.at[o], {"sp": sp_peer(o)})
        for o in range(1, n_sp)
    ]
    for copy in mod_copies:
        copy.start()

    def lat_copy(k, s, relay):
        if not relay:
            return remote(
                lat_hbm.at[s], lat_all.at[k, s], lat_s.at[k, s], lat_r.at[k, s], {"tp": peer[k]}
            )
        via, to = (1, 2) if s == 0 else (2, 1)
        return remote(
            lat_all.at[via, s], lat_all.at[3, s], lat_s.at[3, s], lat_r.at[3, s], {"tp": peer[to]}
        )

    half = rows // 2

    def lat_part(k, s, p):
        part = pl.ds(p * half, half)
        return remote(
            lat_hbm.at[s, part], lat_all.at[k, s, part], early_s.at[k, p], early_r.at[k, p], {"tp": peer[k]}
        )

    lat_part(1, 0, 0).start()
    lat_part(2, 1, 0).start()

    for by_row, by_col, table in ((row_cos, col_cos, cos_ref), (row_sin, col_sin, sin_ref)):
        left = lax.broadcasted_iota(jnp.int32, (GRID_W, HEAD_DIM), 1) < HEAD_DIM // 2
        for r in range(block // GRID_W):
            table[r * GRID_W : (r + 1) * GRID_W, :] = jnp.where(
                left, by_row[r : r + 1, :], by_col[...]
            )

    for copy in mod_copies:
        copy.wait_recv()
    total = mod_p[0]
    for o in range(1, n_sp):
        total = total + mod_p[o]
    mod_all[tp] = total
    all_copies = [
        remote(mod_all.at[tp], mod_all.at[tp], moda_s.at[k], moda_r.at[k], {"tp": peer[k]})
        for k in (1, 2, 3)
    ]
    for copy in all_copies:
        copy.start()
    lat_part(1, 0, 1).start()
    lat_part(2, 1, 1).start()
    lat_copy(1, 1, False).start()
    lat_copy(2, 0, False).start()
    for k in (1, 2, 3):
        remote(
            mod_all.at[peer[k]], mod_all.at[peer[k]], moda_s.at[k], moda_r.at[k], {"tp": peer[k]}
        ).wait_recv()
    for t in range(n_tp):
        cols = slice(t * wid, (t + 1) * wid)
        mod_b[:, cols] = mod_all[t, :, 0:wid]
        mod_a[:, cols] = (1.0 + mod_all[t, :, wid : 2 * wid]) * gain_ref[:, cols]
        mod_g[:, cols] = mod_all[t, :, 2 * wid : 3 * wid]

    def norm_rows(src, mod_row, base, count):
        a_row = mod_a[pl.ds(mod_row, 1), :]
        b_row = mod_b[pl.ds(mod_row, 1), :]

        @pl.loop(0, count // CHUNK, unroll=4)
        def _(c):
            at = pl.multiple_of(c * CHUNK, CHUNK)
            x = src[pl.ds(at, CHUNK), :].astype(F32)
            inv = lax.rsqrt(jnp.mean(x * x, axis=-1, keepdims=True) + EPSILON)
            hbuf[pl.ds(base + at, CHUNK), :] = (x * inv * a_row + b_row).astype(BF16)

    for i in (3, 4, 5):
        loads[i].wait()
    ctx_at = pl.multiple_of(sp * lc, lc)

    @pl.loop(0, samples)
    def _(s):
        norm_rows(ctx_v.at[s], samples, 0, lc)
        ckv[s, pl.ds(ctx_at, lc), :] = jnp.dot(
            hbuf[0:lc, :], wqkv[:, qw : qw + 2 * kw], preferred_element_type=F32
        ).astype(BF16)

    mine = ckv.at[:, pl.ds(ctx_at, lc), :]
    ctx_copies = [
        remote(mine, mine, ctx_s.at[o], ctx_r.at[o], {"sp": sp_peer(o)}) for o in range(1, n_sp)
    ]
    for copy in ctx_copies:
        copy.start()

    for s in (0, 1):
        lat_part(1 + s, s, 0).wait_recv()
        lat_part(1 + s, s, 1).wait_recv()
        lat_copy(3, s, True).start()

    loads[6].wait()
    loads[7].wait()
    lane = lax.broadcasted_iota(jnp.int32, (rows, HEAD_DIM), 1)
    low = lane % (HEAD_DIM // 2) < HEAD_DIM // 4

    def turn(u, cos, sin):
        other = jnp.where(
            low, pltpu.roll(u, HEAD_DIM - HEAD_DIM // 4, 1), pltpu.roll(u, HEAD_DIM // 4, 1)
        )
        return u * cos + other * sin

    halo_up = remote(
        kvbuf.at[:, pl.ds(block, WINDOW), :],
        kvbuf.at[:, pl.ds(0, WINDOW), :],
        halo_s.at[0],
        halo_r.at[0],
        {"sp": sp_peer(1)},
    )
    halo_down = remote(
        kvbuf.at[:, pl.ds(WINDOW, WINDOW), :],
        kvbuf.at[:, pl.ds(WINDOW + block, WINDOW), :],
        halo_s.at[1],
        halo_r.at[1],
        {"sp": sp_peer(n_sp - 1)},
    )

    @pl.loop(0, n_tp)
    def _(k):
        @pl.when(k == 1)
        def _():
            lat_copy(1, 1, False).wait_recv()

        @pl.when(k == 2)
        def _():
            lat_copy(2, 0, False).wait_recv()

        @pl.when(k == 3)
        def _():
            lat_copy(3, 0, True).wait_recv()
            lat_copy(3, 1, True).wait_recv()

        kx, ky = k % 2, k // 2
        bx = tx + kx - 2 * tx * kx
        by = ty + ky - 2 * ty * ky
        b = 2 * by + bx
        for s in range(samples):
            norm_rows(lat_all.at[k, s], s, s * rows, rows)
        at = pl.multiple_of(b * rows, rows)
        cos = cos_ref[pl.ds(at, rows), :]
        sin = sin_ref[pl.ds(at, rows), :]
        for c in range(heads // 2 + 1):
            prod = jnp.dot(
                hbuf[0 : samples * rows, :], wqkv[:, c * 2 * HEAD_DIM : (c + 1) * 2 * HEAD_DIM], preferred_element_type=F32
            )
            for s in range(samples):
                part = prod[s * rows : (s + 1) * rows]
                first = turn(part[:, :HEAD_DIM], cos, sin).astype(BF16)
                if c < heads // 2:
                    second = turn(part[:, HEAD_DIM:], cos, sin).astype(BF16)
                    qbuf[s, b, 2 * c * rows : (2 * c + 1) * rows, :] = first
                    qbuf[s, b, (2 * c + 1) * rows : (2 * c + 2) * rows, :] = second
                else:
                    kvbuf[s, pl.ds(WINDOW + at, rows), 0:HEAD_DIM] = first
                    kvbuf[s, pl.ds(WINDOW + at, rows), HEAD_DIM:] = part[:, HEAD_DIM:].astype(BF16)

        @pl.when(b == 0)
        def _():
            halo_down.start()

        @pl.when(b == n_tp - 1)
        def _():
            halo_up.start()

    loads[8].wait()
    for o in range(1, n_sp):
        got = ckv.at[:, pl.ds(pl.multiple_of(sp_peer(n_sp - o) * lc, lc), lc), :]
        remote(got, got, ctx_s.at[o], ctx_r.at[o], {"sp": sp_peer(o)}).wait_recv()

    scale = HEAD_DIM ** (-0.5) * LOG2E
    seq = block * n_sp
    nums = (((1,), (1,)), ((), ()))

    def rs_copy(i):
        return remote(
            psend.at[i], rs.at[i], rs_s.at[i], rs_r.at[i], {"tp": peer[TARGETS[i]]}
        )

    def pick(i, which):
        value = SENDS[-1][which]
        for j in range(len(SENDS) - 1):
            value = jnp.where(i == j, SENDS[j][which], value)
        return value

    span = 3 * WINDOW
    pair = 2 * rows
    row_id = lax.broadcasted_iota(jnp.int32, (pair, 1), 0)

    @pl.loop(0, 8)
    def _(i):
        k = pick(i, 0)
        s = pick(i, 1)
        kx, ky = k % 2, k // 2
        b = 2 * (ty + ky - 2 * ty * ky) + tx + kx - 2 * tx * kx
        at = pl.multiple_of(b * rows, rows)
        fresh = (i == 0) | (i == 2) | (i == 3) | (i == 6)

        @pl.when(fresh & (b == 0))
        def _():
            halo_up.wait_recv()

        @pl.when(fresh & (b == n_tp - 1))
        def _():
            halo_down.wait_recv()

        kc = ckv[s, :, 0:HEAD_DIM]
        vc = ckv[s, :, HEAD_DIM:]
        kl = kvbuf[s, pl.ds(at, span), 0:HEAD_DIM]
        vl = kvbuf[s, pl.ds(at, span), HEAD_DIM:]
        key = lax.broadcasted_iota(jnp.int32, (pair, span), 1)
        query = lax.broadcasted_iota(jnp.int32, (pair, span), 0) % rows
        pos = key + (sp * block + b * rows - WINDOW)
        allowed = (key >= query) & (key <= query + 2 * WINDOW) & (pos >= 0) & (pos < seq)
        for c in range(heads // 2):
            q = qbuf[s, b, c * pair : (c + 1) * pair, :]
            sc = lax.dot_general(q, kc, nums, preferred_element_type=F32)
            sl = lax.dot_general(q, kl, nums, preferred_element_type=F32)
            sl = jnp.where(allowed, sl, NEGATIVE)
            sink2 = jnp.where(row_id < rows, sink_ref[0, 2 * c], sink_ref[0, 2 * c + 1]) * LOG2E
            top = jnp.maximum(
                jnp.max(sc, axis=-1, keepdims=True), jnp.max(sl, axis=-1, keepdims=True)
            )
            top = jnp.maximum(top * scale, sink2)
            ec = jnp.exp2(sc * scale - top)
            el = jnp.exp2(sl * scale - top)
            total = (
                jnp.sum(ec, axis=-1, keepdims=True)
                + jnp.sum(el, axis=-1, keepdims=True)
                + jnp.exp2(sink2 - top)
            )
            o = jnp.dot(ec.astype(BF16), vc, preferred_element_type=F32)
            o = o + jnp.dot(el.astype(BF16), vl, preferred_element_type=F32)
            o = (o / total).astype(BF16)
            abuf[:, 2 * c * HEAD_DIM : (2 * c + 1) * HEAD_DIM] = o[:rows]
            abuf[:, (2 * c + 1) * HEAD_DIM : (2 * c + 2) * HEAD_DIM] = o[rows:]
        for n in range(n_tp):
            cols = slice(n * wid, (n + 1) * wid)
            psend[i, :, cols] = jnp.dot(
                abuf[...], wo[:, cols], preferred_element_type=F32
            ).astype(BF16)

        for j in range(4):

            @pl.when(i == j)
            def _(j=j):
                rs_copy(j).start()

        for j in (4, 5):

            @pl.when(i == j)
            def _(j=j):
                rs_copy(j - 4).wait_recv()

                @pl.loop(0, rows // CHUNK)
                def _(r):
                    part = pl.ds(pl.multiple_of(r * CHUNK, CHUNK), CHUNK)
                    psend[j, part, :] = (
                        psend[j, part, :].astype(F32) + rs[j - 4, part, :].astype(F32)
                    ).astype(BF16)

                rs_copy(j).start()

    for s in range(2):
        rs_copy(2 + s).wait_recv()
        rs_copy(4 + s).wait_recv()
        g_row = mod_g[s : s + 1, :]

        @pl.loop(0, rows // CHUNK, unroll=2)
        def _(r, s=s, g_row=g_row):
            part = pl.ds(pl.multiple_of(r * CHUNK, CHUNK), CHUNK)
            branch = (
                psend[6 + s, part, :].astype(F32)
                + rs[2 + s, part, :].astype(F32)
                + rs[4 + s, part, :].astype(F32)
            )
            out_ref[s, part, :] = (
                lat_all[0, s, part, :].astype(F32) + g_row * branch
            ).astype(BF16)

    for copy in mod_copies + all_copies + ctx_copies:
        copy.wait_send()
    for k, s in ((1, 1), (2, 0)):
        lat_copy(k, s, False).wait_send()
        lat_part(k, k - 1, 0).wait_send()
        lat_part(k, k - 1, 1).wait_send()
    for s in (0, 1):
        lat_copy(3, s, True).wait_send()
    halo_up.wait_send()
    halo_down.wait_send()
    for i in range(6):
        rs_copy(i).wait_send()


def local(
    n_sp,
    n_tp,
    latent,
    context,
    condition,
    ctx_condition,
    norm_gain,
    w_shift,
    w_scale,
    w_gate,
    w_query,
    w_key,
    w_value,
    w_out,
    sink,
):
    rows, samples, width = latent.shape
    lc = context.shape[0]
    wid = w_shift.shape[1]
    depth = w_shift.shape[0]
    qw, kw = w_query.shape[1], w_key.shape[1]
    heads = qw // HEAD_DIM
    block = rows * n_tp
    assert n_tp == 4 and samples == 2 and kw == HEAD_DIM and rows == WINDOW and block % GRID_W == 0 and heads % 2 == 0
    quarter = HEAD_DIM // 4
    lane = jnp.arange(HEAD_DIM, dtype=jnp.int32)
    freqs = 10000.0 ** (-(lane % quarter).astype(F32) / quarter)
    sign = jnp.where(lane % (2 * quarter) < quarter, -1.0, 1.0).astype(F32)
    grid_rows = block // GRID_W
    first = lax.axis_index("sp") * grid_rows

    def table(position):
        angle = position.astype(F32)[:, None] * freqs[None, :]
        return jnp.cos(angle), jnp.sin(angle) * sign[None, :]

    row_table = table(first + jnp.arange(grid_rows, dtype=jnp.int32))
    col_table = table(jnp.arange(GRID_W, dtype=jnp.int32))
    hbm = pl.BlockSpec(memory_space=pl.ANY)
    vmem = pl.BlockSpec(memory_space=pltpu.VMEM)
    smem = pl.BlockSpec(memory_space=pltpu.SMEM)
    dma = pltpu.SemaphoreType.DMA
    mixed = pl.pallas_call(
        functools.partial(kernel, n_sp),
        out_shape=jax.ShapeDtypeStruct((samples, rows, width), BF16),
        in_specs=[hbm, hbm, vmem, vmem, vmem, hbm, hbm, hbm, hbm, hbm, hbm, hbm, smem, vmem, vmem, vmem, vmem],
        out_specs=vmem,
        scratch_shapes=[
            pltpu.VMEM((n_tp, samples, rows, width), BF16),
            pltpu.VMEM((samples, lc, width), BF16),
            pltpu.VMEM((3, depth, wid), BF16),
            pltpu.VMEM((width, qw + 2 * kw), BF16),
            pltpu.VMEM((qw, width), BF16),
            pltpu.VMEM((8, depth), F32),
            pltpu.VMEM((n_sp, 8, 3 * wid), F32),
            pltpu.VMEM((n_tp, 8, 3 * wid), F32),
            pltpu.VMEM((8, width), F32),
            pltpu.VMEM((8, width), F32),
            pltpu.VMEM((8, width), F32),
            pltpu.VMEM((max(samples * rows, lc), width), BF16),
            pltpu.VMEM((samples, n_tp, heads * rows, HEAD_DIM), BF16),
            pltpu.VMEM((samples, block + 2 * WINDOW, 2 * kw), BF16),
            pltpu.VMEM((samples, lc * n_sp, 2 * kw), BF16),
            pltpu.VMEM((rows, qw), BF16),
            pltpu.VMEM((block, HEAD_DIM), F32),
            pltpu.VMEM((block, HEAD_DIM), F32),
            pltpu.VMEM((8, rows, width), BF16),
            pltpu.VMEM((6, rows, width), BF16),
            dma((9,)),
            dma((n_sp,)),
            dma((n_sp,)),
            dma((n_tp,)),
            dma((n_tp,)),
            dma((n_tp, 2)),
            dma((n_tp, 2)),
            dma((n_tp, 2)),
            dma((n_tp, 2)),
            dma((n_sp,)),
            dma((n_sp,)),
            dma((2,)),
            dma((2,)),
            dma((6,)),
            dma((6,)),
        ],
        compiler_params=pltpu.CompilerParams(
            collective_id=0, has_side_effects=True, vmem_limit_bytes=60 * 1024 * 1024
        ),
        name="step",
    )(
        latent.transpose(1, 0, 2),
        context.transpose(1, 0, 2),
        condition,
        ctx_condition,
        norm_gain[None],
        w_shift,
        w_scale,
        w_gate,
        w_query,
        w_key,
        w_value,
        w_out,
        sink[None],
        *row_table,
        *col_table,
    )
    return mixed.transpose(1, 0, 2)


def solution(mesh):
    return jax.shard_map(
        functools.partial(local, mesh.shape["sp"], mesh.shape["tp"]),
        mesh=mesh,
        in_specs=(
            P(("sp", "tp"), "dp", None),
            P("sp", "dp", None),
            P("dp", "sp"),
            P("sp"),
            P(),
            P("sp", "tp"),
            P("sp", "tp"),
            P("sp", "tp"),
            P(None, "tp"),
            P(None, "tp"),
            P(None, "tp"),
            P("tp", None),
            P("tp"),
        ),
        out_specs=P(("sp", "tp"), "dp", None),
        check_vma=False,
    )
```

profile of v0, /device:TPU:0, one launch (start us, length us, event | category | flops | bytes accessed | tf_op | source)
XLA Modules:
  0.0 97.1 jit_solution(4480815051383462764)
XLA Ops:
  0.0 0.0 copy-start
  0.0 0.7 fusion.1
  0.7 0.8 fusion
  1.5 2.5 %copy.20 = bf16[128,2,2048]{2,0,1:T(8,128)(2,1)} copy(bf16[128,2,2048]{2,1,0:T(2,128)(2,1)} %param.13) | data formatting | bytes 2097152 | tf_op args[0]
  4.1 0.0 copy-done
  4.1 2.2 %copy.19 = bf16[256,2,2048]{2,0,1:T(8,128)(2,1)} copy(bf16[256,2,2048]{2,1,0:T(2,128)(2,1)S(1)} %copy-done) | data formatting | bytes 4194304 | tf_op args[1]
  6.3 87.5 %step.1 = bf16[2,128,2048]{2,1,0:T(8,128)(2,1)} custom-call(bf16[2,128,2048]{2,1,0:T(8,128)(2,1)} %bitcast.11, bf16[2,256,2048]{2,1,0:T(8,128)(2,1)} %bitcast.9, bf16[2,512]{1,0:T(2,128)(2,1)} %cond_ref.1, bf16[512]{0:T(512)(128)(2,1)} %cctx_ref.1, f32[1,2048]{1,0:T(1,128)} %bitcast.12, bf16[512,512]{1,0:T(8,128)(2,1)} %wsh_hbm.1, bf16[512,512]{1,0:T(8,128)(2,1)} %wsc_hbm.1, ...), custom_call_target="tpu_custom_call" | custom-call | tf_op jit(solution)/shard_map/step/pallas_call | solution.py:472
  93.8 3.3 %copy.16 = bf16[128,2,2048]{2,1,0:T(2,128)(2,1)} copy(bf16[128,2,2048]{2,0,1:T(8,128)(2,1)} %bitcast.10) | data formatting | bytes 2097152 | tf_op jit(solution)/shard_map/transpose | solution.py:535
  (3 shorter events, 0.0 us)
Async XLA Ops:
  0.0 4.1 %copy-start = (bf16[256,2,2048]{2,1,0:T(2,128)(2,1)S(1)}, bf16[256,2,2048]{2,1,0:T(2,128)(2,1)}, u32[]{:S(2)}) copy-start(bf16[256,2,2048]{2,1,0:T(2,128)(2,1)} %param.14) | copy-start | bytes 6291460
where the time goes:
time: 97.3 us; the launch traced here: 97.1 us
  Pallas kernels  87.5 us (90%)
  local copies, waits for them, and re-layouts  8.03 us (8%)
  other arithmetic  1.54 us (2%)
    pallas_call x1, Pallas kernels, local(): pl.pallas_call(functools.partial(kernel, n_sp), out_shape=jax.ShapeDtypeS...  87.5 us
    unnamed x4, local copies, waits for them, and re-layouts  4.76 us
    transpose x1, local copies, waits for them, and re-layouts, local(): return mixed.transpose(1, 0, 2)  3.27 us

commit v1 on v0

--- a/solution.py
+++ b/solution.py
@@ -3,6 +3,7 @@
 
 import jax
 import jax.numpy as jnp
+import numpy as np
 from jax import lax
 from jax.experimental import pallas as pl
 from jax.experimental.pallas import tpu as pltpu
@@ -42,6 +43,7 @@
     col_cos,
     col_sin,
     out_ref,
+    lat_raw,
     lat_all,
     ctx_v,
     wmod,
@@ -79,13 +81,13 @@
     rs_s,
     rs_r,
 ):
-    samples, rows, width = lat_hbm.shape
+    rows, samples, width = lat_hbm.shape
     n_tp = mod_all.shape[0]
     wid = wmod.shape[2]
     qw = wq_hbm.shape[1]
     kw = wk_hbm.shape[1]
     heads = qw // HEAD_DIM
-    lc = ctx_hbm.shape[1]
+    lc = ctx_hbm.shape[0]
     block = rows * n_tp
     sp = lax.axis_index("sp")
     tp = lax.axis_index("tp")
@@ -102,24 +104,58 @@
         pltpu.make_async_copy(ctx_hbm, ctx_v, loc_sem.at[3]),
         pltpu.make_async_copy(wk_hbm, wqkv.at[:, pl.ds(qw, kw)], loc_sem.at[4]),
         pltpu.make_async_copy(wv_hbm, wqkv.at[:, pl.ds(qw + kw, kw)], loc_sem.at[5]),
-        pltpu.make_async_copy(lat_hbm, lat_all.at[0], loc_sem.at[6]),
+        pltpu.make_async_copy(lat_hbm, lat_raw, loc_sem.at[6]),
         pltpu.make_async_copy(wq_hbm, wqkv.at[:, pl.ds(0, qw)], loc_sem.at[7]),
         pltpu.make_async_copy(wo_hbm, wo, loc_sem.at[8]),
     ]
-    for load in loads:
-        load.start()
+    for i in (6, 0, 1, 2, 3, 4, 5, 7, 8):
+        loads[i].start()
 
     barrier = pltpu.get_barrier_semaphore()
     for o in range(1, n_sp):
         pl.semaphore_signal(barrier, inc=1, device_id={"sp": sp_peer(o)}, device_id_type=MESH)
     for k in (1, 2, 3):
         pl.semaphore_signal(barrier, inc=1, device_id={"tp": peer[k]}, device_id_type=MESH)
+
+    def apart(src, at):
+        return jnp.swapaxes(src[pl.ds(at, CHUNK)], 0, 1)
+
+    loads[6].wait()
+
+    @pl.loop(0, rows // CHUNK)
+    def _(c):
+        at = pl.multiple_of(c * CHUNK, CHUNK)
+        both = apart(lat_raw, at)
+        for s in range(samples):
+            lat_all[0, s, pl.ds(at, CHUNK), :] = both[s]
+
     pl.semaphore_wait(barrier, n_sp - 1 + n_tp - 1)
 
     def remote(src, dst, ssem, rsem, dev):
         return pltpu.make_async_remote_copy(
             src_ref=src, dst_ref=dst, send_sem=ssem, recv_sem=rsem, device_id=dev, device_id_type=MESH
         )
+
+    def lat_copy(k, s, relay):
+        if not relay:
+            return remote(
+                lat_all.at[0, s], lat_all.at[k, s], lat_s.at[k, s], lat_r.at[k, s], {"tp": peer[k]}
+            )
+        via, to = (1, 2) if s == 0 else (2, 1)
+        return remote(
+            lat_all.at[via, s], lat_all.at[3, s], lat_s.at[3, s], lat_r.at[3, s], {"tp": peer[to]}
+        )
+
+    half = rows // 2
+
+    def lat_part(k, s, p):
+        part = pl.ds(p * half, half)
+        return remote(
+            lat_all.at[0, s, part], lat_all.at[k, s, part], early_s.at[k, p], early_r.at[k, p], {"tp": peer[k]}
+        )
+
+    lat_part(1, 0, 0).start()
+    lat_part(2, 1, 0).start()
 
     act_s[...] = jnp.zeros_like(act_s)
     cv = cond_ref[...].astype(F32)
@@ -137,32 +173,12 @@
     for copy in mod_copies:
         copy.start()
 
-    def lat_copy(k, s, relay):
-        if not relay:
-            return remote(
-                lat_hbm.at[s], lat_all.at[k, s], lat_s.at[k, s], lat_r.at[k, s], {"tp": peer[k]}
-            )
-        via, to = (1, 2) if s == 0 else (2, 1)
-        return remote(
-            lat_all.at[via, s], lat_all.at[3, s], lat_s.at[3, s], lat_r.at[3, s], {"tp": peer[to]}
-        )
-
-    half = rows // 2
-
-    def lat_part(k, s, p):
-        part = pl.ds(p * half, half)
-        return remote(
-            lat_hbm.at[s, part], lat_all.at[k, s, part], early_s.at[k, p], early_r.at[k, p], {"tp": peer[k]}
-        )
-
-    lat_part(1, 0, 0).start()
-    lat_part(2, 1, 0).start()
-
+    grid_rows = block // GRID_W
     for by_row, by_col, table in ((row_cos, col_cos, cos_ref), (row_sin, col_sin, sin_ref)):
         left = lax.broadcasted_iota(jnp.int32, (GRID_W, HEAD_DIM), 1) < HEAD_DIM // 2
-        for r in range(block // GRID_W):
+        for r in range(grid_rows):
             table[r * GRID_W : (r + 1) * GRID_W, :] = jnp.where(
-                left, by_row[r : r + 1, :], by_col[...]
+                left, by_row[pl.ds(sp * grid_rows + r, 1), :], by_col[...]
             )
 
     for copy in mod_copies:
@@ -191,27 +207,31 @@
         mod_a[:, cols] = (1.0 + mod_all[t, :, wid : 2 * wid]) * gain_ref[:, cols]
         mod_g[:, cols] = mod_all[t, :, 2 * wid : 3 * wid]
 
+    def modulate(values, mod_row):
+        x = values.astype(F32)
+        inv = lax.rsqrt(jnp.mean(x * x, axis=-1, keepdims=True) + EPSILON)
+        return (x * inv * mod_a[mod_row : mod_row + 1, :] + mod_b[mod_row : mod_row + 1, :]).astype(BF16)
+
     def norm_rows(src, mod_row, base, count):
-        a_row = mod_a[pl.ds(mod_row, 1), :]
-        b_row = mod_b[pl.ds(mod_row, 1), :]
-
         @pl.loop(0, count // CHUNK, unroll=4)
         def _(c):
             at = pl.multiple_of(c * CHUNK, CHUNK)
-            x = src[pl.ds(at, CHUNK), :].astype(F32)
-            inv = lax.rsqrt(jnp.mean(x * x, axis=-1, keepdims=True) + EPSILON)
-            hbuf[pl.ds(base + at, CHUNK), :] = (x * inv * a_row + b_row).astype(BF16)
+            hbuf[pl.ds(base + at, CHUNK), :] = modulate(src[pl.ds(at, CHUNK), :], mod_row)
 
     for i in (3, 4, 5):
         loads[i].wait()
     ctx_at = pl.multiple_of(sp * lc, lc)
 
-    @pl.loop(0, samples)
-    def _(s):
-        norm_rows(ctx_v.at[s], samples, 0, lc)
-        ckv[s, pl.ds(ctx_at, lc), :] = jnp.dot(
-            hbuf[0:lc, :], wqkv[:, qw : qw + 2 * kw], preferred_element_type=F32
-        ).astype(BF16)
+    @pl.loop(0, lc // CHUNK, unroll=2)
+    def _(c):
+        at = pl.multiple_of(c * CHUNK, CHUNK)
+        both = apart(ctx_v, at)
+        for s in range(samples):
+            hbuf[pl.ds(s * lc + at, CHUNK), :] = modulate(both[s], samples)
+
+    made = jnp.dot(hbuf[...], wqkv[:, qw : qw + 2 * kw], preferred_element_type=F32).astype(BF16)
+    for s in range(samples):
+        ckv[s, pl.ds(ctx_at, lc), :] = made[s * lc : (s + 1) * lc]
 
     mine = ckv.at[:, pl.ds(ctx_at, lc), :]
     ctx_copies = [
@@ -225,7 +245,6 @@
         lat_part(1 + s, s, 1).wait_recv()
         lat_copy(3, s, True).start()
 
-    loads[6].wait()
     loads[7].wait()
     lane = lax.broadcasted_iota(jnp.int32, (rows, HEAD_DIM), 1)
     low = lane % (HEAD_DIM // 2) < HEAD_DIM // 4
@@ -399,19 +418,19 @@
     for s in range(2):
         rs_copy(2 + s).wait_recv()
         rs_copy(4 + s).wait_recv()
-        g_row = mod_g[s : s + 1, :]
-
-        @pl.loop(0, rows // CHUNK, unroll=2)
-        def _(r, s=s, g_row=g_row):
-            part = pl.ds(pl.multiple_of(r * CHUNK, CHUNK), CHUNK)
+
+    @pl.loop(0, rows // CHUNK, unroll=2)
+    def _(r):
+        part = pl.ds(pl.multiple_of(r * CHUNK, CHUNK), CHUNK)
+        both = []
+        for s in range(samples):
             branch = (
                 psend[6 + s, part, :].astype(F32)
                 + rs[2 + s, part, :].astype(F32)
                 + rs[4 + s, part, :].astype(F32)
             )
-            out_ref[s, part, :] = (
-                lat_all[0, s, part, :].astype(F32) + g_row * branch
-            ).astype(BF16)
+            both.append((lat_all[0, s, part, :].astype(F32) + mod_g[s : s + 1, :] * branch).astype(BF16))
+        out_ref[part] = jnp.swapaxes(jnp.stack(both), 0, 1)
 
     for copy in mod_copies + all_copies + ctx_copies:
         copy.wait_send()
@@ -453,30 +472,29 @@
     block = rows * n_tp
     assert n_tp == 4 and samples == 2 and kw == HEAD_DIM and rows == WINDOW and block % GRID_W == 0 and heads % 2 == 0
     quarter = HEAD_DIM // 4
-    lane = jnp.arange(HEAD_DIM, dtype=jnp.int32)
-    freqs = 10000.0 ** (-(lane % quarter).astype(F32) / quarter)
-    sign = jnp.where(lane % (2 * quarter) < quarter, -1.0, 1.0).astype(F32)
-    grid_rows = block // GRID_W
-    first = lax.axis_index("sp") * grid_rows
-
-    def table(position):
-        angle = position.astype(F32)[:, None] * freqs[None, :]
-        return jnp.cos(angle), jnp.sin(angle) * sign[None, :]
-
-    row_table = table(first + jnp.arange(grid_rows, dtype=jnp.int32))
-    col_table = table(jnp.arange(GRID_W, dtype=jnp.int32))
+    lane = np.arange(HEAD_DIM)
+    freqs = 10000.0 ** (-(lane % quarter).astype(np.float32) / quarter)
+    sign = np.where(lane % (2 * quarter) < quarter, -1.0, 1.0)
+
+    def table(count):
+        angle = np.arange(count, dtype=np.float32)[:, None] * freqs[None, :].astype(np.float32)
+        return jnp.asarray(np.cos(angle), F32), jnp.asarray(np.sin(angle) * sign[None, :], F32)
+
+    row_table = table(n_sp * block // GRID_W)
+    col_table = table(GRID_W)
     hbm = pl.BlockSpec(memory_space=pl.ANY)
     vmem = pl.BlockSpec(memory_space=pltpu.VMEM)
     smem = pl.BlockSpec(memory_space=pltpu.SMEM)
     dma = pltpu.SemaphoreType.DMA
     mixed = pl.pallas_call(
         functools.partial(kernel, n_sp),
-        out_shape=jax.ShapeDtypeStruct((samples, rows, width), BF16),
+        out_shape=jax.ShapeDtypeStruct((rows, samples, width), BF16),
         in_specs=[hbm, hbm, vmem, vmem, vmem, hbm, hbm, hbm, hbm, hbm, hbm, hbm, smem, vmem, vmem, vmem, vmem],
         out_specs=vmem,
         scratch_shapes=[
+            pltpu.VMEM((rows, samples, width), BF16),
             pltpu.VMEM((n_tp, samples, rows, width), BF16),
-            pltpu.VMEM((samples, lc, width), BF16),
+            pltpu.VMEM((lc, samples, width), BF16),
             pltpu.VMEM((3, depth, wid), BF16),
             pltpu.VMEM((width, qw + 2 * kw), BF16),
             pltpu.VMEM((qw, width), BF16),
@@ -486,7 +504,7 @@
             pltpu.VMEM((8, width), F32),
             pltpu.VMEM((8, width), F32),
             pltpu.VMEM((8, width), F32),
-            pltpu.VMEM((max(samples * rows, lc), width), BF16),
+            pltpu.VMEM((samples * max(rows, lc), width), BF16),
             pltpu.VMEM((samples, n_tp, heads * rows, HEAD_DIM), BF16),
             pltpu.VMEM((samples, block + 2 * WINDOW, 2 * kw), BF16),
             pltpu.VMEM((samples, lc * n_sp, 2 * kw), BF16),
@@ -516,8 +534,8 @@
         ),
         name="step",
     )(
-        latent.transpose(1, 0, 2),
-        context.transpose(1, 0, 2),
+        latent,
+        context,
         condition,
         ctx_condition,
         norm_gain[None],
@@ -532,7 +550,7 @@
         *row_table,
         *col_table,
     )
-    return mixed.transpose(1, 0, 2)
+    return mixed
 
 
 def solution(mesh):

time: 97.3 us -> 90.1 us (0.926)
  local copies, waits for them, and re-layouts: 8.03 us -> 2.92 us
  other arithmetic: 1.54 us -> 0 us
    transpose x1 -> x0, local copies, waits for them, and re-layouts: 3.27 us -> none  [local(): return mixed.transpose(1, 0, 2)]
    unnamed x4 -> x1, local copies, waits for them, and re-layouts: 4.76 us -> 2.92 us
    mul x2 -> x0, other arithmetic: 1.53 us -> none  [table(): return (jnp.cos(angle), jnp.sin(angle) * sign[None, :])]
where the time goes in v1:
time: 90.1 us; the launch traced here: 89.9 us
  Pallas kernels  86.9 us (96%)
  local copies, waits for them, and re-layouts  2.92 us (3%)
    pallas_call x1, Pallas kernels, local(): pl.pallas_call(functools.partial(kernel, n_sp), out_shape=jax.ShapeDtypeS...  86.9 us
    unnamed x1, local copies, waits for them, and re-layouts  2.92 us

profile of v1, /device:TPU:0, one launch (start us, length us, event | category | flops | bytes accessed | tf_op | source)
XLA Modules:
  0.0 89.9 jit_solution(3713564291131394982)
XLA Ops:
  0.0 86.9 %step.1 = bf16[128,2,2048]{2,1,0:T(2,128)(2,1)} custom-call(bf16[128,2,2048]{2,1,0:T(2,128)(2,1)} %lat_hbm.1, bf16[256,2,2048]{2,1,0:T(2,128)(2,1)} %ctx_hbm.1, bf16[2,512]{1,0:T(2,128)(2,1)} %cond_ref.1, bf16[512]{0:T(512)(128)(2,1)} %cctx_ref.1, f32[1,2048]{1,0:T(1,128)} %bitcast.2, bf16[512,512]{1,0:T(8,128)(2,1)} %wsh_hbm.1, bf16[512,512]{1,0:T(8,128)(2,1)} %wsc_hbm.1, ...), custom_call_target="tpu_custom_call" | custom-call | tf_op jit(solution)/shard_map/step/pallas_call | solution.py:489
  87.0 2.9 %copy.19 = bf16[128,2,2048]{2,1,0:T(2,128)(2,1)} copy(bf16[128,2,2048]{2,1,0:T(2,128)(2,1)} %step.1) | data formatting | bytes 2097152

commit v2 on v1

--- a/solution.py
+++ b/solution.py
@@ -19,8 +19,6 @@
 BF16 = jnp.bfloat16
 LOG2E = math.log2(math.e)
 CHUNK = 16
-SENDS = ((3, 0), (3, 1), (1, 0), (2, 1), (2, 0), (1, 1), (0, 0), (0, 1))
-TARGETS = (1, 2, 1, 2, 2, 1)
 
 
 def kernel(
@@ -48,7 +46,7 @@
     ctx_v,
     wmod,
     wqkv,
-    wo,
+    wo_all,
     act_s,
     mod_p,
     mod_all,
@@ -59,12 +57,10 @@
     qbuf,
     kvbuf,
     ckv,
-    abuf,
+    attn,
+    acc,
     cos_ref,
     sin_ref,
-    psend,
-    rs,
-
     loc_sem,
     modp_s,
     modp_r,
@@ -72,14 +68,24 @@
     moda_r,
     lat_s,
     lat_r,
-    early_s,
-    early_r,
+    relay_s,
+    relay_r,
     ctx_s,
     ctx_r,
     halo_s,
     halo_r,
-    rs_s,
-    rs_r,
+    attn_s,
+    attn_r,
+    wo_s,
+    wo_r,
+    wod_s,
+    wod_r,
+    woz_s,
+    woz_r,
+    woc_s,
+    woc_r,
+    woe_s,
+    woe_r,
 ):
     rows, samples, width = lat_hbm.shape
     n_tp = mod_all.shape[0]
@@ -91,6 +97,7 @@
     block = rows * n_tp
     sp = lax.axis_index("sp")
     tp = lax.axis_index("tp")
+    dp = lax.axis_index("dp")
     tx, ty = tp % 2, tp // 2
     peer = {1: 2 * ty + 1 - tx, 2: 2 * (1 - ty) + tx, 3: 3 - tp}
 
@@ -106,7 +113,7 @@
         pltpu.make_async_copy(wv_hbm, wqkv.at[:, pl.ds(qw + kw, kw)], loc_sem.at[5]),
         pltpu.make_async_copy(lat_hbm, lat_raw, loc_sem.at[6]),
         pltpu.make_async_copy(wq_hbm, wqkv.at[:, pl.ds(0, qw)], loc_sem.at[7]),
-        pltpu.make_async_copy(wo_hbm, wo, loc_sem.at[8]),
+        pltpu.make_async_copy(wo_hbm, wo_all.at[0], loc_sem.at[8]),
     ]
     for i in (6, 0, 1, 2, 3, 4, 5, 7, 8):
         loads[i].start()
@@ -116,6 +123,8 @@
         pl.semaphore_signal(barrier, inc=1, device_id={"sp": sp_peer(o)}, device_id_type=MESH)
     for k in (1, 2, 3):
         pl.semaphore_signal(barrier, inc=1, device_id={"tp": peer[k]}, device_id_type=MESH)
+
+    pl.semaphore_signal(barrier, inc=1, device_id={"dp": 1 - dp}, device_id_type=MESH)
 
     def apart(src, at):
         return jnp.swapaxes(src[pl.ds(at, CHUNK)], 0, 1)
@@ -129,33 +138,59 @@
         for s in range(samples):
             lat_all[0, s, pl.ds(at, CHUNK), :] = both[s]
 
-    pl.semaphore_wait(barrier, n_sp - 1 + n_tp - 1)
+    pl.semaphore_wait(barrier, n_sp - 1 + n_tp)
 
     def remote(src, dst, ssem, rsem, dev):
         return pltpu.make_async_remote_copy(
             src_ref=src, dst_ref=dst, send_sem=ssem, recv_sem=rsem, device_id=dev, device_id_type=MESH
         )
 
-    def lat_copy(k, s, relay):
-        if not relay:
-            return remote(
-                lat_all.at[0, s], lat_all.at[k, s], lat_s.at[k, s], lat_r.at[k, s], {"tp": peer[k]}
-            )
-        via, to = (1, 2) if s == 0 else (2, 1)
-        return remote(
-            lat_all.at[via, s], lat_all.at[3, s], lat_s.at[3, s], lat_r.at[3, s], {"tp": peer[to]}
-        )
-
     half = rows // 2
 
-    def lat_part(k, s, p):
+    def direct(k, s, p):
         part = pl.ds(p * half, half)
         return remote(
-            lat_all.at[0, s, part], lat_all.at[k, s, part], early_s.at[k, p], early_r.at[k, p], {"tp": peer[k]}
+            lat_all.at[0, s, part], lat_all.at[k, s, part], lat_s.at[k, s, p], lat_r.at[k, s, p], {"tp": peer[k]}
         )
 
-    lat_part(1, 0, 0).start()
-    lat_part(2, 1, 0).start()
+    def relay(s, p):
+        part = pl.ds(p * half, half)
+        return remote(
+            lat_all.at[1 + p, s, part], lat_all.at[3, s, part], relay_s.at[s, p], relay_r.at[s, p], {"tp": peer[2 - p]}
+        )
+
+    zh = sp % 2
+    quarter = qw // 4
+    mine_q = 2 * zh + dp
+    pair_q = 2 * (1 - zh) + dp
+
+    def wo_rows(index, count=quarter, skip=0):
+        return pl.ds(pl.multiple_of(index * quarter + skip, count), count)
+
+    def wo_direct(k):
+        part = wo_rows(mine_q)
+        return remote(wo_hbm.at[part], wo_all.at[k, part], wo_s.at[k], wo_r.at[k], {"tp": peer[k]})
+
+    def wo_relay(p):
+        part = wo_rows(mine_q, quarter // 2, p * (quarter // 2))
+        return remote(
+            wo_all.at[1 + p, part], wo_all.at[3, part], wod_s.at[p], wod_r.at[p], {"tp": peer[2 - p]}
+        )
+
+    def wo_pair(k, index):
+        part = wo_all.at[k, wo_rows(index)]
+        return remote(part, part, woz_s.at[k], woz_r.at[k], {"sp": sp + 1 - 2 * zh})
+
+    def wo_core(k, index):
+        part = wo_all.at[k, wo_rows(index)]
+        return remote(part, part, woc_s.at[k], woc_r.at[k], {"dp": 1 - dp})
+
+    def wo_last(k, index):
+        part = wo_all.at[k, wo_rows(index)]
+        return remote(part, part, woe_s.at[k], woe_r.at[k], {"dp": 1 - dp})
+
+    direct(1, 0, 0).start()
+    direct(2, 0, 1).start()
 
     act_s[...] = jnp.zeros_like(act_s)
     cv = cond_ref[...].astype(F32)
@@ -193,10 +228,18 @@
     ]
     for copy in all_copies:
         copy.start()
-    lat_part(1, 0, 1).start()
-    lat_part(2, 1, 1).start()
-    lat_copy(1, 1, False).start()
-    lat_copy(2, 0, False).start()
+    direct(1, 0, 1).start()
+    direct(2, 0, 0).start()
+    direct(1, 0, 0).wait_recv()
+    direct(2, 0, 1).wait_recv()
+    relay(0, 0).start()
+    relay(0, 1).start()
+    wo_direct(1).start()
+    wo_direct(2).start()
+    direct(1, 1, 0).start()
+    direct(2, 1, 1).start()
+    direct(1, 1, 1).start()
+    direct(2, 1, 0).start()
     for k in (1, 2, 3):
         remote(
             mod_all.at[peer[k]], mod_all.at[peer[k]], moda_s.at[k], moda_r.at[k], {"tp": peer[k]}
@@ -210,7 +253,8 @@
     def modulate(values, mod_row):
         x = values.astype(F32)
         inv = lax.rsqrt(jnp.mean(x * x, axis=-1, keepdims=True) + EPSILON)
-        return (x * inv * mod_a[mod_row : mod_row + 1, :] + mod_b[mod_row : mod_row + 1, :]).astype(BF16)
+        row = pl.ds(mod_row, 1)
+        return (x * inv * mod_a[row, :] + mod_b[row, :]).astype(BF16)
 
     def norm_rows(src, mod_row, base, count):
         @pl.loop(0, count // CHUNK, unroll=4)
@@ -240,11 +284,6 @@
     for copy in ctx_copies:
         copy.start()
 
-    for s in (0, 1):
-        lat_part(1 + s, s, 0).wait_recv()
-        lat_part(1 + s, s, 1).wait_recv()
-        lat_copy(3, s, True).start()
-
     loads[7].wait()
     lane = lax.broadcasted_iota(jnp.int32, (rows, HEAD_DIM), 1)
     low = lane % (HEAD_DIM // 2) < HEAD_DIM // 4
@@ -255,108 +294,106 @@
         )
         return u * cos + other * sin
 
-    halo_up = remote(
-        kvbuf.at[:, pl.ds(block, WINDOW), :],
-        kvbuf.at[:, pl.ds(0, WINDOW), :],
-        halo_s.at[0],
-        halo_r.at[0],
-        {"sp": sp_peer(1)},
-    )
-    halo_down = remote(
-        kvbuf.at[:, pl.ds(WINDOW, WINDOW), :],
-        kvbuf.at[:, pl.ds(WINDOW + block, WINDOW), :],
-        halo_s.at[1],
-        halo_r.at[1],
-        {"sp": sp_peer(n_sp - 1)},
-    )
-
-    @pl.loop(0, n_tp)
-    def _(k):
-        @pl.when(k == 1)
-        def _():
-            lat_copy(1, 1, False).wait_recv()
-
-        @pl.when(k == 2)
-        def _():
-            lat_copy(2, 0, False).wait_recv()
-
-        @pl.when(k == 3)
-        def _():
-            lat_copy(3, 0, True).wait_recv()
-            lat_copy(3, 1, True).wait_recv()
-
-        kx, ky = k % 2, k // 2
-        bx = tx + kx - 2 * tx * kx
-        by = ty + ky - 2 * ty * ky
-        b = 2 * by + bx
-        for s in range(samples):
-            norm_rows(lat_all.at[k, s], s, s * rows, rows)
-        at = pl.multiple_of(b * rows, rows)
-        cos = cos_ref[pl.ds(at, rows), :]
-        sin = sin_ref[pl.ds(at, rows), :]
-        for c in range(heads // 2 + 1):
-            prod = jnp.dot(
-                hbuf[0 : samples * rows, :], wqkv[:, c * 2 * HEAD_DIM : (c + 1) * 2 * HEAD_DIM], preferred_element_type=F32
-            )
-            for s in range(samples):
-                part = prod[s * rows : (s + 1) * rows]
-                first = turn(part[:, :HEAD_DIM], cos, sin).astype(BF16)
-                if c < heads // 2:
-                    second = turn(part[:, HEAD_DIM:], cos, sin).astype(BF16)
-                    qbuf[s, b, 2 * c * rows : (2 * c + 1) * rows, :] = first
-                    qbuf[s, b, (2 * c + 1) * rows : (2 * c + 2) * rows, :] = second
-                else:
-                    kvbuf[s, pl.ds(WINDOW + at, rows), 0:HEAD_DIM] = first
-                    kvbuf[s, pl.ds(WINDOW + at, rows), HEAD_DIM:] = part[:, HEAD_DIM:].astype(BF16)
-
-        @pl.when(b == 0)
-        def _():
-            halo_down.start()
-
-        @pl.when(b == n_tp - 1)
-        def _():
-            halo_up.start()
-
-    loads[8].wait()
-    for o in range(1, n_sp):
-        got = ckv.at[:, pl.ds(pl.multiple_of(sp_peer(n_sp - o) * lc, lc), lc), :]
-        remote(got, got, ctx_s.at[o], ctx_r.at[o], {"sp": sp_peer(o)}).wait_recv()
+    def halo_up(s):
+        return remote(
+            kvbuf.at[s, pl.ds(block, WINDOW), :],
+            kvbuf.at[s, pl.ds(0, WINDOW), :],
+            halo_s.at[0, s],
+            halo_r.at[0, s],
+            {"sp": lax.min(sp + 1, n_sp - 1)},
+        )
+
+    def halo_down(s):
+        return remote(
+            kvbuf.at[s, pl.ds(WINDOW, WINDOW), :],
+            kvbuf.at[s, pl.ds(WINDOW + block, WINDOW), :],
+            halo_s.at[1, s],
+            halo_r.at[1, s],
+            {"sp": lax.max(sp - 1, 0)},
+        )
+
+    not_first, not_last = sp > 0, sp < n_sp - 1
+
+    @pl.when(sp == 0)
+    def _():
+        kvbuf[:, 0:WINDOW, :] = jnp.zeros((samples, WINDOW, 2 * kw), BF16)
+
+    @pl.when(sp == n_sp - 1)
+    def _():
+        kvbuf[:, WINDOW + block :, :] = jnp.zeros((samples, WINDOW, 2 * kw), BF16)
+
+    acc[...] = jnp.zeros_like(acc)
+
+    def attn_copy(k, s, dest):
+        return remote(attn.at[n_tp + k, s], attn.at[k, s], attn_s.at[k, s], attn_r.at[k, s], {"tp": dest})
+
+    def project(s):
+        @pl.loop(0, n_tp // 2)
+        def _(j):
+            @pl.when(j == 0)
+            def _():
+                direct(1, s, 1).wait_recv()
+
+            @pl.when(j == 1)
+            def _():
+                direct(2, s, 0).wait_recv()
+                relay(s, 0).wait_recv()
+                relay(s, 1).wait_recv()
+
+            by = ty + j - 2 * ty * j
+            spots = []
+            for e in range(2):
+                norm_rows(lat_all.at[2 * j + e, s], s, e * rows, rows)
+                b = 2 * by + (1 - tx if e else tx)
+                at = pl.multiple_of(b * rows, rows)
+                spots.append((b, at, cos_ref[pl.ds(at, rows), :], sin_ref[pl.ds(at, rows), :]))
+            for c in range(heads // 2 + 1):
+                prod = jnp.dot(
+                    hbuf[0 : 2 * rows, :],
+                    wqkv[:, c * 2 * HEAD_DIM : (c + 1) * 2 * HEAD_DIM],
+                    preferred_element_type=F32,
+                )
+                for e, (b, at, cos, sin) in enumerate(spots):
+                    part = prod[e * rows : (e + 1) * rows]
+                    first = turn(part[:, :HEAD_DIM], cos, sin).astype(BF16)
+                    if c < heads // 2:
+                        second = turn(part[:, HEAD_DIM:], cos, sin).astype(BF16)
+                        qbuf[s, b, 2 * c * rows : (2 * c + 1) * rows, :] = first
+                        qbuf[s, b, (2 * c + 1) * rows : (2 * c + 2) * rows, :] = second
+                    else:
+                        kvbuf[s, pl.ds(WINDOW + at, rows), 0:HEAD_DIM] = first
+                        kvbuf[s, pl.ds(WINDOW + at, rows), HEAD_DIM:] = part[:, HEAD_DIM:].astype(BF16)
+
+        @pl.when(not_last)
+        def _():
+            halo_up(s).start()
+
+        @pl.when(not_first)
+        def _():
+            halo_down(s).start()
 
     scale = HEAD_DIM ** (-0.5) * LOG2E
     seq = block * n_sp
     nums = (((1,), (1,)), ((), ()))
 
-    def rs_copy(i):
-        return remote(
-            psend.at[i], rs.at[i], rs_s.at[i], rs_r.at[i], {"tp": peer[TARGETS[i]]}
-        )
-
-    def pick(i, which):
-        value = SENDS[-1][which]
-        for j in range(len(SENDS) - 1):
-            value = jnp.where(i == j, SENDS[j][which], value)
-        return value
-
     span = 3 * WINDOW
     pair = 2 * rows
     row_id = lax.broadcasted_iota(jnp.int32, (pair, 1), 0)
 
-    @pl.loop(0, 8)
-    def _(i):
-        k = pick(i, 0)
-        s = pick(i, 1)
-        kx, ky = k % 2, k // 2
-        b = 2 * (ty + ky - 2 * ty * ky) + tx + kx - 2 * tx * kx
+    def attend(i, s):
+        b = jnp.where(i < 2, i + 1, (i - 2) * (n_tp - 1))
+        bx, by = b % 2, b // 2
+        k = 2 * (by + ty - 2 * by * ty) + bx + tx - 2 * bx * tx
         at = pl.multiple_of(b * rows, rows)
-        fresh = (i == 0) | (i == 2) | (i == 3) | (i == 6)
-
-        @pl.when(fresh & (b == 0))
-        def _():
-            halo_up.wait_recv()
-
-        @pl.when(fresh & (b == n_tp - 1))
-        def _():
-            halo_down.wait_recv()
+        slot = jnp.where(k == 0, 0, n_tp + k)
+
+        @pl.when((b == 0) & not_first)
+        def _():
+            halo_up(s).wait_recv()
+
+        @pl.when((b == n_tp - 1) & not_last)
+        def _():
+            halo_down(s).wait_recv()
 
         kc = ckv[s, :, 0:HEAD_DIM]
         vc = ckv[s, :, HEAD_DIM:]
@@ -386,64 +423,112 @@
             o = jnp.dot(ec.astype(BF16), vc, preferred_element_type=F32)
             o = o + jnp.dot(el.astype(BF16), vl, preferred_element_type=F32)
             o = (o / total).astype(BF16)
-            abuf[:, 2 * c * HEAD_DIM : (2 * c + 1) * HEAD_DIM] = o[:rows]
-            abuf[:, (2 * c + 1) * HEAD_DIM : (2 * c + 2) * HEAD_DIM] = o[rows:]
-        for n in range(n_tp):
-            cols = slice(n * wid, (n + 1) * wid)
-            psend[i, :, cols] = jnp.dot(
-                abuf[...], wo[:, cols], preferred_element_type=F32
-            ).astype(BF16)
-
-        for j in range(4):
-
-            @pl.when(i == j)
-            def _(j=j):
-                rs_copy(j).start()
-
-        for j in (4, 5):
-
-            @pl.when(i == j)
-            def _(j=j):
-                rs_copy(j - 4).wait_recv()
-
-                @pl.loop(0, rows // CHUNK)
-                def _(r):
-                    part = pl.ds(pl.multiple_of(r * CHUNK, CHUNK), CHUNK)
-                    psend[j, part, :] = (
-                        psend[j, part, :].astype(F32) + rs[j - 4, part, :].astype(F32)
-                    ).astype(BF16)
-
-                rs_copy(j).start()
-
-    for s in range(2):
-        rs_copy(2 + s).wait_recv()
-        rs_copy(4 + s).wait_recv()
+            attn[slot, s, :, 2 * c * HEAD_DIM : (2 * c + 1) * HEAD_DIM] = o[:rows]
+            attn[slot, s, :, (2 * c + 1) * HEAD_DIM : (2 * c + 2) * HEAD_DIM] = o[rows:]
+
+        @pl.when((s == 1) & (k > 0))
+        def _():
+            attn_copy(k, s, b).start()
+
+        @pl.when((s == 1) & (i == 1))
+        def _():
+            for p in range(2):
+                wo_relay(p).wait_recv()
+            wo_pair(3, mine_q).start()
+            wo_core(3, mine_q).start()
+
+    @pl.loop(0, samples)
+    def _(s):
+        project(s)
+
+        @pl.when(s == 0)
+        def _():
+            for o in range(1, n_sp):
+                got = ckv.at[:, pl.ds(pl.multiple_of(sp_peer(n_sp - o) * lc, lc), lc), :]
+                remote(got, got, ctx_s.at[o], ctx_r.at[o], {"sp": sp_peer(o)}).wait_recv()
+            for k in (1, 2):
+                wo_direct(k).wait_recv()
+                wo_pair(k, mine_q).start()
+                wo_core(k, mine_q).start()
+
+        @pl.loop(0, n_tp)
+        def _(i):
+            attend(i, s)
+
+        @pl.when(s == 0)
+        def _():
+            direct(1, 1, 0).wait_recv()
+            direct(2, 1, 1).wait_recv()
+            for p in range(2):
+                relay(1, p).start()
+            for p in range(2):
+                wo_relay(p).start()
+            for k in (3, 2, 1):
+                attn_copy(k, 0, peer[k]).start()
+
+    loads[8].wait()
+
+    def hand_over(k):
+        wo_pair(k, pair_q).wait_recv()
+        wo_last(k, pair_q).start()
+
+    def project_out(k):
+        if k > 0:
+            wo_core(k, mine_q + 1 - 2 * dp).wait_recv()
+            wo_last(k, pair_q + 1 - 2 * dp).wait_recv()
+            for s in range(samples):
+                attn_copy(k, s, peer[k]).wait_recv()
+
+        @pl.loop(0, n_tp)
+        def _(n):
+            cols = pl.ds(pl.multiple_of(n * wid, wid), wid)
+            part = jnp.dot(
+                attn[k].reshape(samples * rows, qw), wo_all[k, :, cols], preferred_element_type=F32
+            )
+            acc[:, cols] = acc[:, cols] + part.astype(BF16).astype(F32)
+
+    hand_over(1)
+    hand_over(2)
+    project_out(0)
+    project_out(1)
+    project_out(2)
+    hand_over(3)
+    project_out(3)
 
     @pl.loop(0, rows // CHUNK, unroll=2)
     def _(r):
         part = pl.ds(pl.multiple_of(r * CHUNK, CHUNK), CHUNK)
         both = []
         for s in range(samples):
-            branch = (
-                psend[6 + s, part, :].astype(F32)
-                + rs[2 + s, part, :].astype(F32)
-                + rs[4 + s, part, :].astype(F32)
-            )
+            branch = acc[pl.ds(pl.multiple_of(s * rows + r * CHUNK, CHUNK), CHUNK), :]
             both.append((lat_all[0, s, part, :].astype(F32) + mod_g[s : s + 1, :] * branch).astype(BF16))
         out_ref[part] = jnp.swapaxes(jnp.stack(both), 0, 1)
 
     for copy in mod_copies + all_copies + ctx_copies:
         copy.wait_send()
-    for k, s in ((1, 1), (2, 0)):
-        lat_copy(k, s, False).wait_send()
-        lat_part(k, k - 1, 0).wait_send()
-        lat_part(k, k - 1, 1).wait_send()
-    for s in (0, 1):
-        lat_copy(3, s, True).wait_send()
-    halo_up.wait_send()
-    halo_down.wait_send()
-    for i in range(6):
-        rs_copy(i).wait_send()
+    for s in range(samples):
+        for p in range(2):
+            direct(1, s, p).wait_send()
+            direct(2, s, p).wait_send()
+            relay(s, p).wait_send()
+        for k in (1, 2, 3):
+            attn_copy(k, s, peer[k]).wait_send()
+
+        @pl.when(not_last)
+        def _(s=s):
+            halo_up(s).wait_send()
+
+        @pl.when(not_first)
+        def _(s=s):
+            halo_down(s).wait_send()
+
+    for p in range(2):
+        wo_direct(1 + p).wait_send()
+        wo_relay(p).wait_send()
+    for k in (1, 2, 3):
+        wo_pair(k, mine_q).wait_send()
+        wo_core(k, mine_q).wait_send()
+        wo_last(k, pair_q).wait_send()
 
 
 def local(
@@ -470,7 +555,7 @@
     qw, kw = w_query.shape[1], w_key.shape[1]
     heads = qw // HEAD_DIM
     block = rows * n_tp
-    assert n_tp == 4 and samples == 2 and kw == HEAD_DIM and rows == WINDOW and block % GRID_W == 0 and heads % 2 == 0
+    assert n_tp == 4 and n_sp % 2 == 0 and qw % 64 == 0 and samples == 2 and kw == HEAD_DIM and rows == WINDOW and block % GRID_W == 0 and heads % 2 == 0
     quarter = HEAD_DIM // 4
     lane = np.arange(HEAD_DIM)
     freqs = 10000.0 ** (-(lane % quarter).astype(np.float32) / quarter)
@@ -497,7 +582,7 @@
             pltpu.VMEM((lc, samples, width), BF16),
             pltpu.VMEM((3, depth, wid), BF16),
             pltpu.VMEM((width, qw + 2 * kw), BF16),
-            pltpu.VMEM((qw, width), BF16),
+            pltpu.VMEM((n_tp, qw, width), BF16),
             pltpu.VMEM((8, depth), F32),
             pltpu.VMEM((n_sp, 8, 3 * wid), F32),
             pltpu.VMEM((n_tp, 8, 3 * wid), F32),
@@ -508,26 +593,35 @@
             pltpu.VMEM((samples, n_tp, heads * rows, HEAD_DIM), BF16),
             pltpu.VMEM((samples, block + 2 * WINDOW, 2 * kw), BF16),
             pltpu.VMEM((samples, lc * n_sp, 2 * kw), BF16),
-            pltpu.VMEM((rows, qw), BF16),
+            pltpu.VMEM((2 * n_tp, samples, rows, qw), BF16),
+            pltpu.VMEM((samples * rows, width), F32),
             pltpu.VMEM((block, HEAD_DIM), F32),
             pltpu.VMEM((block, HEAD_DIM), F32),
-            pltpu.VMEM((8, rows, width), BF16),
-            pltpu.VMEM((6, rows, width), BF16),
             dma((9,)),
             dma((n_sp,)),
             dma((n_sp,)),
             dma((n_tp,)),
             dma((n_tp,)),
-            dma((n_tp, 2)),
-            dma((n_tp, 2)),
-            dma((n_tp, 2)),
-            dma((n_tp, 2)),
+            dma((n_tp, samples, 2)),
+            dma((n_tp, samples, 2)),
+            dma((samples, 2)),
+            dma((samples, 2)),
             dma((n_sp,)),
             dma((n_sp,)),
+            dma((2, samples)),
+            dma((2, samples)),
+            dma((n_tp, samples)),
+            dma((n_tp, samples)),
+            dma((n_tp,)),
+            dma((n_tp,)),
             dma((2,)),
             dma((2,)),
-            dma((6,)),
-            dma((6,)),
+            dma((n_tp,)),
+            dma((n_tp,)),
+            dma((n_tp,)),
+            dma((n_tp,)),
+            dma((n_tp,)),
+            dma((n_tp,)),
         ],
         compiler_params=pltpu.CompilerParams(
             collective_id=0, has_side_effects=True, vmem_limit_bytes=60 * 1024 * 1024

time: 90.1 us -> 86.8 us (0.963); the launches traced: 89.9 us -> 85.2 us
  Pallas kernels: 86.9 us -> 82.3 us
    pallas_call x1, Pallas kernels: 86.9 us -> 82.3 us  [local(): pl.pallas_call(functools.partial(kernel, n_sp), out_shape=jax.ShapeDtypeS...]
where the time goes in v2:
time: 86.8 us; the launch traced here: 85.2 us
  Pallas kernels  82.3 us (95%)
  local copies, waits for them, and re-layouts  2.92 us (3%)
    pallas_call x1, Pallas kernels, local(): pl.pallas_call(functools.partial(kernel, n_sp), out_shape=jax.ShapeDtypeS...  82.3 us
    unnamed x1, local copies, waits for them, and re-layouts  2.92 us

profile of v2, /device:TPU:0, one launch (start us, length us, event | category | flops | bytes accessed | tf_op | source)
XLA Modules:
  0.0 85.2 jit_solution(12016412777708726327)
XLA Ops:
  0.0 82.3 %step.1 = bf16[128,2,2048]{2,1,0:T(2,128)(2,1)} custom-call(bf16[128,2,2048]{2,1,0:T(2,128)(2,1)} %lat_hbm.1, bf16[256,2,2048]{2,1,0:T(2,128)(2,1)} %ctx_hbm.1, bf16[2,512]{1,0:T(2,128)(2,1)} %cond_ref.1, bf16[512]{0:T(512)(128)(2,1)} %cctx_ref.1, f32[1,2048]{1,0:T(1,128)} %bitcast.2, bf16[512,512]{1,0:T(8,128)(2,1)} %wsh_hbm.1, bf16[512,512]{1,0:T(8,128)(2,1)} %wsc_hbm.1, ...), custom_call_target="tpu_custom_call" | custom-call | tf_op jit(solution)/shard_map/step/pallas_call | solution.py:574
  82.3 2.9 %copy.19 = bf16[128,2,2048]{2,1,0:T(2,128)(2,1)} copy(bf16[128,2,2048]{2,1,0:T(2,128)(2,1)} %step.1) | data formatting | bytes 2097152

commit v3 on v2

--- a/solution.py
+++ b/solution.py
@@ -40,7 +40,8 @@
     row_sin,
     col_cos,
     col_sin,
-    out_ref,
+    out_hbm,
+    mixed,
     lat_raw,
     lat_all,
     ctx_v,
@@ -86,6 +87,7 @@
     woc_r,
     woe_s,
     woe_r,
+    out_sem,
 ):
     rows, samples, width = lat_hbm.shape
     n_tp = mod_all.shape[0]
@@ -115,7 +117,7 @@
         pltpu.make_async_copy(wq_hbm, wqkv.at[:, pl.ds(0, qw)], loc_sem.at[7]),
         pltpu.make_async_copy(wo_hbm, wo_all.at[0], loc_sem.at[8]),
     ]
-    for i in (6, 0, 1, 2, 3, 4, 5, 7, 8):
+    for i in (0, 1, 2, 6, 3, 4, 5, 7, 8):
         loads[i].start()
 
     barrier = pltpu.get_barrier_semaphore()
@@ -129,15 +131,6 @@
     def apart(src, at):
         return jnp.swapaxes(src[pl.ds(at, CHUNK)], 0, 1)
 
-    loads[6].wait()
-
-    @pl.loop(0, rows // CHUNK)
-    def _(c):
-        at = pl.multiple_of(c * CHUNK, CHUNK)
-        both = apart(lat_raw, at)
-        for s in range(samples):
-            lat_all[0, s, pl.ds(at, CHUNK), :] = both[s]
-
     pl.semaphore_wait(barrier, n_sp - 1 + n_tp)
 
     def remote(src, dst, ssem, rsem, dev):
@@ -167,30 +160,37 @@
     def wo_rows(index, count=quarter, skip=0):
         return pl.ds(pl.multiple_of(index * quarter + skip, count), count)
 
-    def wo_direct(k):
-        part = wo_rows(mine_q)
-        return remote(wo_hbm.at[part], wo_all.at[k, part], wo_s.at[k], wo_r.at[k], {"tp": peer[k]})
+    def wo_half(index, p):
+        return wo_rows(index, quarter // 2, p * (quarter // 2))
+
+    def wo_direct(k, p):
+        part = wo_half(mine_q, p)
+        return remote(wo_hbm.at[part], wo_all.at[k, part], wo_s.at[k, p], wo_r.at[k, p], {"tp": peer[k]})
 
     def wo_relay(p):
-        part = wo_rows(mine_q, quarter // 2, p * (quarter // 2))
+        part = wo_half(mine_q, p)
         return remote(
             wo_all.at[1 + p, part], wo_all.at[3, part], wod_s.at[p], wod_r.at[p], {"tp": peer[2 - p]}
         )
 
-    def wo_pair(k, index):
-        part = wo_all.at[k, wo_rows(index)]
-        return remote(part, part, woz_s.at[k], woz_r.at[k], {"sp": sp + 1 - 2 * zh})
-
-    def wo_core(k, index):
-        part = wo_all.at[k, wo_rows(index)]
-        return remote(part, part, woc_s.at[k], woc_r.at[k], {"dp": 1 - dp})
+    def wo_pair(k, p, index):
+        part = wo_all.at[k, wo_half(index, p)]
+        return remote(part, part, woz_s.at[k, p], woz_r.at[k, p], {"sp": sp + 1 - 2 * zh})
+
+    def wo_core(k, p, index):
+        part = wo_all.at[k, wo_half(index, p)]
+        return remote(part, part, woc_s.at[k, p], woc_r.at[k, p], {"dp": 1 - dp})
+
+    def wo_share(k, p):
+        wo_pair(k, p, mine_q).start()
+        wo_core(k, p, mine_q).start()
 
     def wo_last(k, index):
         part = wo_all.at[k, wo_rows(index)]
         return remote(part, part, woe_s.at[k], woe_r.at[k], {"dp": 1 - dp})
 
-    direct(1, 0, 0).start()
-    direct(2, 0, 1).start()
+    wo_direct(1, 0).start()
+    wo_direct(2, 1).start()
 
     act_s[...] = jnp.zeros_like(act_s)
     cv = cond_ref[...].astype(F32)
@@ -200,13 +200,22 @@
     both = act_s[...].astype(BF16)
     for m in range(3):
         loads[m].wait()
-        mod_p[0, :, m * wid : (m + 1) * wid] = jnp.dot(both, wmod[m], preferred_element_type=F32)
+        mod_p[0, :, m * wid : (m + 1) * wid] = jnp.dot(both, wmod[m], preferred_element_type=F32)[0:4]
     mod_copies = [
         remote(mod_p.at[0], mod_p.at[o], modp_s.at[o], modp_r.at[o], {"sp": sp_peer(o)})
         for o in range(1, n_sp)
     ]
     for copy in mod_copies:
         copy.start()
+
+    loads[6].wait()
+
+    @pl.loop(0, rows // CHUNK)
+    def _(c):
+        at = pl.multiple_of(c * CHUNK, CHUNK)
+        both = apart(lat_raw, at)
+        for s in range(samples):
+            lat_all[0, s, pl.ds(at, CHUNK), :] = both[s]
 
     grid_rows = block // GRID_W
     for by_row, by_col, table in ((row_cos, col_cos, cos_ref), (row_sin, col_sin, sin_ref)):
@@ -228,18 +237,16 @@
     ]
     for copy in all_copies:
         copy.start()
+    wo_direct(1, 1).start()
+    wo_direct(2, 0).start()
+    direct(1, 0, 0).start()
+    direct(2, 0, 1).start()
     direct(1, 0, 1).start()
     direct(2, 0, 0).start()
-    direct(1, 0, 0).wait_recv()
-    direct(2, 0, 1).wait_recv()
-    relay(0, 0).start()
-    relay(0, 1).start()
-    wo_direct(1).start()
-    wo_direct(2).start()
-    direct(1, 1, 0).start()
-    direct(2, 1, 1).start()
-    direct(1, 1, 1).start()
-    direct(2, 1, 0).start()
+    wo_direct(1, 0).wait_recv()
+    wo_direct(2, 1).wait_recv()
+    wo_share(1, 0)
+    wo_share(2, 1)
     for k in (1, 2, 3):
         remote(
             mod_all.at[peer[k]], mod_all.at[peer[k]], moda_s.at[k], moda_r.at[k], {"tp": peer[k]}
@@ -283,6 +290,19 @@
     ]
     for copy in ctx_copies:
         copy.start()
+
+    wo_direct(1, 1).wait_recv()
+    wo_direct(2, 0).wait_recv()
+    direct(1, 0, 0).wait_recv()
+    direct(2, 0, 1).wait_recv()
+    for p in range(2):
+        relay(0, p).start()
+    for p in range(2):
+        wo_relay(p).start()
+    direct(1, 1, 0).start()
+    direct(2, 1, 1).start()
+    direct(1, 1, 1).start()
+    direct(2, 1, 0).start()
 
     loads[7].wait()
     lane = lax.broadcasted_iota(jnp.int32, (rows, HEAD_DIM), 1)
@@ -364,13 +384,13 @@
                         kvbuf[s, pl.ds(WINDOW + at, rows), 0:HEAD_DIM] = first
                         kvbuf[s, pl.ds(WINDOW + at, rows), HEAD_DIM:] = part[:, HEAD_DIM:].astype(BF16)
 
-        @pl.when(not_last)
-        def _():
-            halo_up(s).start()
-
-        @pl.when(not_first)
-        def _():
-            halo_down(s).start()
+            @pl.when(not_last & (by == 1))
+            def _():
+                halo_up(s).start()
+
+            @pl.when(not_first & (by == 0))
+            def _():
+                halo_down(s).start()
 
     scale = HEAD_DIM ** (-0.5) * LOG2E
     seq = block * n_sp
@@ -381,9 +401,9 @@
     row_id = lax.broadcasted_iota(jnp.int32, (pair, 1), 0)
 
     def attend(i, s):
-        b = jnp.where(i < 2, i + 1, (i - 2) * (n_tp - 1))
-        bx, by = b % 2, b // 2
-        k = 2 * (by + ty - 2 * by * ty) + bx + tx - 2 * bx * tx
+        k = n_tp - 1 - i
+        kx, ky = k % 2, k // 2
+        b = 2 * (ty + ky - 2 * ty * ky) + tx + kx - 2 * tx * kx
         at = pl.multiple_of(b * rows, rows)
         slot = jnp.where(k == 0, 0, n_tp + k)
 
@@ -430,26 +450,24 @@
         def _():
             attn_copy(k, s, b).start()
 
-        @pl.when((s == 1) & (i == 1))
-        def _():
-            for p in range(2):
-                wo_relay(p).wait_recv()
-            wo_pair(3, mine_q).start()
-            wo_core(3, mine_q).start()
-
     @pl.loop(0, samples)
     def _(s):
         project(s)
 
         @pl.when(s == 0)
         def _():
+            wo_share(1, 1)
+            wo_share(2, 0)
             for o in range(1, n_sp):
                 got = ckv.at[:, pl.ds(pl.multiple_of(sp_peer(n_sp - o) * lc, lc), lc), :]
                 remote(got, got, ctx_s.at[o], ctx_r.at[o], {"sp": sp_peer(o)}).wait_recv()
-            for k in (1, 2):
-                wo_direct(k).wait_recv()
-                wo_pair(k, mine_q).start()
-                wo_core(k, mine_q).start()
+            wo_relay(0).wait_recv()
+            wo_share(3, 0)
+
+        @pl.when(s == 1)
+        def _():
+            wo_relay(1).wait_recv()
+            wo_share(3, 1)
 
         @pl.loop(0, n_tp)
         def _(i):
@@ -461,20 +479,20 @@
             direct(2, 1, 1).wait_recv()
             for p in range(2):
                 relay(1, p).start()
-            for p in range(2):
-                wo_relay(p).start()
             for k in (3, 2, 1):
                 attn_copy(k, 0, peer[k]).start()
 
     loads[8].wait()
 
     def hand_over(k):
-        wo_pair(k, pair_q).wait_recv()
+        for p in range(2):
+            wo_pair(k, p, pair_q).wait_recv()
         wo_last(k, pair_q).start()
 
     def project_out(k):
         if k > 0:
-            wo_core(k, mine_q + 1 - 2 * dp).wait_recv()
+            for p in range(2):
+                wo_core(k, p, mine_q + 1 - 2 * dp).wait_recv()
             wo_last(k, pair_q + 1 - 2 * dp).wait_recv()
             for s in range(samples):
                 attn_copy(k, s, peer[k]).wait_recv()
@@ -485,24 +503,30 @@
             part = jnp.dot(
                 attn[k].reshape(samples * rows, qw), wo_all[k, :, cols], preferred_element_type=F32
             )
-            acc[:, cols] = acc[:, cols] + part.astype(BF16).astype(F32)
+            total = acc[:, cols] + part.astype(BF16).astype(F32)
+            if k != 1:
+                acc[:, cols] = total
+            else:
+                both = []
+                for s in range(samples):
+                    branch = total[s * rows : (s + 1) * rows]
+                    both.append(
+                        (lat_all[0, s, :, cols].astype(F32) + mod_g[s : s + 1, cols] * branch).astype(BF16)
+                    )
+                mixed[:, :, cols] = jnp.swapaxes(jnp.stack(both), 0, 1)
+                out_copy(n).start()
+
+    def out_copy(n):
+        cols = pl.ds(pl.multiple_of(n * wid, wid), wid)
+        return pltpu.make_async_copy(mixed.at[:, :, cols], out_hbm.at[:, :, cols], out_sem.at[n])
 
     hand_over(1)
     hand_over(2)
     project_out(0)
-    project_out(1)
-    project_out(2)
     hand_over(3)
     project_out(3)
-
-    @pl.loop(0, rows // CHUNK, unroll=2)
-    def _(r):
-        part = pl.ds(pl.multiple_of(r * CHUNK, CHUNK), CHUNK)
-        both = []
-        for s in range(samples):
-            branch = acc[pl.ds(pl.multiple_of(s * rows + r * CHUNK, CHUNK), CHUNK), :]
-            both.append((lat_all[0, s, part, :].astype(F32) + mod_g[s : s + 1, :] * branch).astype(BF16))
-        out_ref[part] = jnp.swapaxes(jnp.stack(both), 0, 1)
+    project_out(2)
+    project_out(1)
 
     for copy in mod_copies + all_copies + ctx_copies:
         copy.wait_send()
@@ -523,12 +547,16 @@
             halo_down(s).wait_send()
 
     for p in range(2):
-        wo_direct(1 + p).wait_send()
+        wo_direct(1, p).wait_send()
+        wo_direct(2, p).wait_send()
         wo_relay(p).wait_send()
+        for k in (1, 2, 3):
+            wo_pair(k, p, mine_q).wait_send()
+            wo_core(k, p, mine_q).wait_send()
     for k in (1, 2, 3):
-        wo_pair(k, mine_q).wait_send()
-        wo_core(k, mine_q).wait_send()
         wo_last(k, pair_q).wait_send()
+    for n in range(n_tp):
+        out_copy(n).wait()
 
 
 def local(
@@ -575,8 +603,9 @@
         functools.partial(kernel, n_sp),
         out_shape=jax.ShapeDtypeStruct((rows, samples, width), BF16),
         in_specs=[hbm, hbm, vmem, vmem, vmem, hbm, hbm, hbm, hbm, hbm, hbm, hbm, smem, vmem, vmem, vmem, vmem],
-        out_specs=vmem,
+        out_specs=hbm,
         scratch_shapes=[
+            pltpu.VMEM((rows, samples, width), BF16),
             pltpu.VMEM((rows, samples, width), BF16),
             pltpu.VMEM((n_tp, samples, rows, width), BF16),
             pltpu.VMEM((lc, samples, width), BF16),
@@ -584,11 +613,11 @@
             pltpu.VMEM((width, qw + 2 * kw), BF16),
             pltpu.VMEM((n_tp, qw, width), BF16),
             pltpu.VMEM((8, depth), F32),
-            pltpu.VMEM((n_sp, 8, 3 * wid), F32),
-            pltpu.VMEM((n_tp, 8, 3 * wid), F32),
-            pltpu.VMEM((8, width), F32),
-            pltpu.VMEM((8, width), F32),
-            pltpu.VMEM((8, width), F32),
+            pltpu.VMEM((n_sp, 4, 3 * wid), F32),
+            pltpu.VMEM((n_tp, 4, 3 * wid), F32),
+            pltpu.VMEM((4, width), F32),
+            pltpu.VMEM((4, width), F32),
+            pltpu.VMEM((4, width), F32),
             pltpu.VMEM((samples * max(rows, lc), width), BF16),
             pltpu.VMEM((samples, n_tp, heads * rows, HEAD_DIM), BF16),
             pltpu.VMEM((samples, block + 2 * WINDOW, 2 * kw), BF16),
@@ -612,13 +641,14 @@
             dma((2, samples)),
             dma((n_tp, samples)),
             dma((n_tp, samples)),
-            dma((n_tp,)),
-            dma((n_tp,)),
+            dma((n_tp, 2)),
+            dma((n_tp, 2)),
             dma((2,)),
             dma((2,)),
-            dma((n_tp,)),
-            dma((n_tp,)),
-            dma((n_tp,)),
+            dma((n_tp, 2)),
+            dma((n_tp, 2)),
+            dma((n_tp, 2)),
+            dma((n_tp, 2)),
             dma((n_tp,)),
             dma((n_tp,)),
             dma((n_tp,)),
@@ -644,7 +674,32 @@
         *row_table,
         *col_table,
     )
-    return mixed
+    pieces = 4
+    piece = rows // pieces
+
+    def hand_out(src, dst, held, sems):
+        def copy(i, out):
+            part = pl.ds(i * piece, piece)
+            if out:
+                return pltpu.make_async_copy(held.at[part], dst.at[part], sems.at[1, i])
+            return pltpu.make_async_copy(src.at[part], held.at[part], sems.at[0, i])
+
+        for i in range(pieces):
+            copy(i, False).start()
+        for i in range(pieces):
+            copy(i, False).wait()
+            copy(i, True).start()
+        for i in range(pieces):
+            copy(i, True).wait()
+
+    return pl.pallas_call(
+        hand_out,
+        out_shape=jax.ShapeDtypeStruct(mixed.shape, BF16),
+        in_specs=[hbm],
+        out_specs=hbm,
+        scratch_shapes=[pltpu.VMEM((rows, samples, width), BF16), dma((2, pieces))],
+        name="hand_out",
+    )(mixed)
 
 
 def solution(mesh):

time: 86.8 us -> 82.5 us (0.950)
  the two profiles are of different devices: /device:TPU:0 before, /device:TPU:3 now
where the time goes in v3:
time: 82.5 us; the launch traced here: 82.3 us
  Pallas kernels  82.3 us (100%)
    pallas_call x1, Pallas kernels, local(): pl.pallas_call(functools.partial(kernel, n_sp), out_shape=jax.ShapeDtypeS...  80.3 us
    pallas_call x1, Pallas kernels, local(): pl.pallas_call(hand_out, out_shape=jax.ShapeDtypeStruct(mixed.shape, BF16...  1.98 us

profile of v3, /device:TPU:3, one launch (start us, length us, event | category | flops | bytes accessed | tf_op | source)
XLA Modules:
  0.0 82.3 jit_solution(2754318406982514607)
XLA Ops:
  0.0 80.3 %step.1.src = bf16[128,2,2048]{2,1,0:T(2,128)(2,1)} custom-call(bf16[128,2,2048]{2,1,0:T(2,128)(2,1)} %lat_hbm.1, bf16[256,2,2048]{2,1,0:T(2,128)(2,1)} %ctx_hbm.1, bf16[2,512]{1,0:T(2,128)(2,1)} %cond_ref.1, bf16[512]{0:T(512)(128)(2,1)} %cctx_ref.1, f32[1,2048]{1,0:T(1,128)} %bitcast.2, bf16[512,512]{1,0:T(8,128)(2,1)} %wsh_hbm.1, ...), custom_call_target="tpu_custom_call" | custom-call | tf_op jit(solution)/shard_map/step/pallas_call | solution.py:602
  80.3 2.0 %hand_out.1 = bf16[128,2,2048]{2,1,0:T(2,128)(2,1)} custom-call(bf16[128,2,2048]{2,1,0:T(2,128)(2,1)} %step.1.src), custom_call_target="tpu_custom_call" | custom-call | tf_op jit(solution)/shard_map/hand_out/pallas_call | solution.py:695

commit v4 on v3

--- a/solution.py
+++ b/solution.py
@@ -19,6 +19,7 @@
 BF16 = jnp.bfloat16
 LOG2E = math.log2(math.e)
 CHUNK = 16
+OUT_PIECES = 2
 
 
 def kernel(
@@ -117,7 +118,7 @@
         pltpu.make_async_copy(wq_hbm, wqkv.at[:, pl.ds(0, qw)], loc_sem.at[7]),
         pltpu.make_async_copy(wo_hbm, wo_all.at[0], loc_sem.at[8]),
     ]
-    for i in (0, 1, 2, 6, 3, 4, 5, 7, 8):
+    for i in (8, 0, 1, 2, 6, 3, 4, 5, 7):
         loads[i].start()
 
     barrier = pltpu.get_barrier_semaphore()
@@ -165,7 +166,7 @@
 
     def wo_direct(k, p):
         part = wo_half(mine_q, p)
-        return remote(wo_hbm.at[part], wo_all.at[k, part], wo_s.at[k, p], wo_r.at[k, p], {"tp": peer[k]})
+        return remote(wo_all.at[0, part], wo_all.at[k, part], wo_s.at[k, p], wo_r.at[k, p], {"tp": peer[k]})
 
     def wo_relay(p):
         part = wo_half(mine_q, p)
@@ -189,6 +190,7 @@
         part = wo_all.at[k, wo_rows(index)]
         return remote(part, part, woe_s.at[k], woe_r.at[k], {"dp": 1 - dp})
 
+    loads[8].wait()
     wo_direct(1, 0).start()
     wo_direct(2, 1).start()
 
@@ -347,50 +349,45 @@
     def attn_copy(k, s, dest):
         return remote(attn.at[n_tp + k, s], attn.at[k, s], attn_s.at[k, s], attn_r.at[k, s], {"tp": dest})
 
-    def project(s):
-        @pl.loop(0, n_tp // 2)
-        def _(j):
-            @pl.when(j == 0)
-            def _():
-                direct(1, s, 1).wait_recv()
-
-            @pl.when(j == 1)
-            def _():
-                direct(2, s, 0).wait_recv()
-                relay(s, 0).wait_recv()
-                relay(s, 1).wait_recv()
-
-            by = ty + j - 2 * ty * j
-            spots = []
-            for e in range(2):
-                norm_rows(lat_all.at[2 * j + e, s], s, e * rows, rows)
-                b = 2 * by + (1 - tx if e else tx)
-                at = pl.multiple_of(b * rows, rows)
-                spots.append((b, at, cos_ref[pl.ds(at, rows), :], sin_ref[pl.ds(at, rows), :]))
-            for c in range(heads // 2 + 1):
-                prod = jnp.dot(
-                    hbuf[0 : 2 * rows, :],
-                    wqkv[:, c * 2 * HEAD_DIM : (c + 1) * 2 * HEAD_DIM],
-                    preferred_element_type=F32,
-                )
-                for e, (b, at, cos, sin) in enumerate(spots):
-                    part = prod[e * rows : (e + 1) * rows]
-                    first = turn(part[:, :HEAD_DIM], cos, sin).astype(BF16)
-                    if c < heads // 2:
-                        second = turn(part[:, HEAD_DIM:], cos, sin).astype(BF16)
-                        qbuf[s, b, 2 * c * rows : (2 * c + 1) * rows, :] = first
-                        qbuf[s, b, (2 * c + 1) * rows : (2 * c + 2) * rows, :] = second
-                    else:
-                        kvbuf[s, pl.ds(WINDOW + at, rows), 0:HEAD_DIM] = first
-                        kvbuf[s, pl.ds(WINDOW + at, rows), HEAD_DIM:] = part[:, HEAD_DIM:].astype(BF16)
-
-            @pl.when(not_last & (by == 1))
-            def _():
-                halo_up(s).start()
-
-            @pl.when(not_first & (by == 0))
-            def _():
-                halo_down(s).start()
+    def project(blocks):
+        spots = []
+        for e, (k, s) in enumerate(blocks):
+            norm_rows(lat_all.at[k, s], s, e * rows, rows)
+            kx, ky = k % 2, k // 2
+            b = 2 * (ty + ky - 2 * ty * ky) + tx + kx - 2 * tx * kx
+            at = pl.multiple_of(b * rows, rows)
+            spots.append((s, b, at, cos_ref[pl.ds(at, rows), :], sin_ref[pl.ds(at, rows), :]))
+        for c in range(heads // 2 + 1):
+            prod = jnp.dot(
+                hbuf[0 : len(blocks) * rows, :],
+                wqkv[:, c * 2 * HEAD_DIM : (c + 1) * 2 * HEAD_DIM],
+                preferred_element_type=F32,
+            )
+            for e, (s, b, at, cos, sin) in enumerate(spots):
+                part = prod[e * rows : (e + 1) * rows]
+                first = turn(part[:, :HEAD_DIM], cos, sin).astype(BF16)
+                if c < heads // 2:
+                    second = turn(part[:, HEAD_DIM:], cos, sin).astype(BF16)
+                    qbuf[s, b, 2 * c * rows : (2 * c + 1) * rows, :] = first
+                    qbuf[s, b, (2 * c + 1) * rows : (2 * c + 2) * rows, :] = second
+                else:
+                    kvbuf[s, pl.ds(WINDOW + at, rows), 0:HEAD_DIM] = first
+                    kvbuf[s, pl.ds(WINDOW + at, rows), HEAD_DIM:] = part[:, HEAD_DIM:].astype(BF16)
+
+    def send_edges(s, bottom, top):
+        @pl.when(not_last & top)
+        def _():
+            halo_up(s).start()
+
+        @pl.when(not_first & bottom)
+        def _():
+            halo_down(s).start()
+
+    at_first, at_last = tp == 0, tp == n_tp - 1
+    inner = (tp > 0) & (tp < n_tp - 1)
+    project([(0, s) for s in range(samples)])
+    for s in range(samples):
+        send_edges(s, at_first, at_last)
 
     scale = HEAD_DIM ** (-0.5) * LOG2E
     seq = block * n_sp
@@ -400,8 +397,13 @@
     pair = 2 * rows
     row_id = lax.broadcasted_iota(jnp.int32, (pair, 1), 0)
 
+    def hand_over(k):
+        for p in range(2):
+            wo_pair(k, p, pair_q).wait_recv()
+        wo_last(k, pair_q).start()
+
     def attend(i, s):
-        k = n_tp - 1 - i
+        k = jnp.where(i == 0, 1, jnp.where(i < n_tp - 1, n_tp - i, 0))
         kx, ky = k % 2, k // 2
         b = 2 * (ty + ky - 2 * ty * ky) + tx + kx - 2 * tx * kx
         at = pl.multiple_of(b * rows, rows)
@@ -452,25 +454,37 @@
 
     @pl.loop(0, samples)
     def _(s):
-        project(s)
-
-        @pl.when(s == 0)
-        def _():
-            wo_share(1, 1)
-            wo_share(2, 0)
-            for o in range(1, n_sp):
-                got = ckv.at[:, pl.ds(pl.multiple_of(sp_peer(n_sp - o) * lc, lc), lc), :]
-                remote(got, got, ctx_s.at[o], ctx_r.at[o], {"sp": sp_peer(o)}).wait_recv()
-            wo_relay(0).wait_recv()
-            wo_share(3, 0)
-
-        @pl.when(s == 1)
-        def _():
-            wo_relay(1).wait_recv()
-            wo_share(3, 1)
+        direct(1, s, 1).wait_recv()
+        direct(2, s, 0).wait_recv()
+        project([(1, s), (2, s)])
+        send_edges(s, inner, inner)
 
         @pl.loop(0, n_tp)
         def _(i):
+            @pl.when(i == s)
+            def _():
+                relay(s, 0).wait_recv()
+                relay(s, 1).wait_recv()
+                project([(3, s)])
+                send_edges(s, at_last, at_first)
+
+                @pl.when(s == 0)
+                def _():
+                    wo_share(1, 1)
+                    wo_share(2, 0)
+                    for o in range(1, n_sp):
+                        got = ckv.at[:, pl.ds(pl.multiple_of(sp_peer(n_sp - o) * lc, lc), lc), :]
+                        remote(got, got, ctx_s.at[o], ctx_r.at[o], {"sp": sp_peer(o)}).wait_recv()
+                    wo_relay(0).wait_recv()
+                    wo_share(3, 0)
+
+                @pl.when(s == 1)
+                def _():
+                    wo_relay(1).wait_recv()
+                    wo_share(3, 1)
+                    hand_over(1)
+                    hand_over(2)
+
             attend(i, s)
 
         @pl.when(s == 0)
@@ -482,13 +496,6 @@
             for k in (3, 2, 1):
                 attn_copy(k, 0, peer[k]).start()
 
-    loads[8].wait()
-
-    def hand_over(k):
-        for p in range(2):
-            wo_pair(k, p, pair_q).wait_recv()
-        wo_last(k, pair_q).start()
-
     def project_out(k):
         if k > 0:
             for p in range(2):
@@ -497,14 +504,14 @@
             for s in range(samples):
                 attn_copy(k, s, peer[k]).wait_recv()
 
-        @pl.loop(0, n_tp)
+        @pl.loop(0, OUT_PIECES)
         def _(n):
-            cols = pl.ds(pl.multiple_of(n * wid, wid), wid)
+            cols = out_cols(n)
             part = jnp.dot(
                 attn[k].reshape(samples * rows, qw), wo_all[k, :, cols], preferred_element_type=F32
             )
             total = acc[:, cols] + part.astype(BF16).astype(F32)
-            if k != 1:
+            if k < n_tp - 1:
                 acc[:, cols] = total
             else:
                 both = []
@@ -516,17 +523,17 @@
                 mixed[:, :, cols] = jnp.swapaxes(jnp.stack(both), 0, 1)
                 out_copy(n).start()
 
+    def out_cols(n):
+        span = width // OUT_PIECES
+        return pl.ds(pl.multiple_of(n * span, span), span)
+
     def out_copy(n):
-        cols = pl.ds(pl.multiple_of(n * wid, wid), wid)
+        cols = out_cols(n)
         return pltpu.make_async_copy(mixed.at[:, :, cols], out_hbm.at[:, :, cols], out_sem.at[n])
 
-    hand_over(1)
-    hand_over(2)
-    project_out(0)
     hand_over(3)
-    project_out(3)
-    project_out(2)
-    project_out(1)
+    for k in range(n_tp):
+        project_out(k)
 
     for copy in mod_copies + all_copies + ctx_copies:
         copy.wait_send()
@@ -555,7 +562,7 @@
             wo_core(k, p, mine_q).wait_send()
     for k in (1, 2, 3):
         wo_last(k, pair_q).wait_send()
-    for n in range(n_tp):
+    for n in range(OUT_PIECES):
         out_copy(n).wait()
 
 
@@ -651,7 +658,7 @@
             dma((n_tp, 2)),
             dma((n_tp,)),
             dma((n_tp,)),
-            dma((n_tp,)),
+            dma((OUT_PIECES,)),
         ],
         compiler_params=pltpu.CompilerParams(
             collective_id=0, has_side_effects=True, vmem_limit_bytes=60 * 1024 * 1024

time: 82.5 us -> 79.6 us (0.965)
  the two profiles are of different devices: /device:TPU:3 before, /device:TPU:0 now
where the time goes in v4:
time: 79.6 us; the launch traced here: 79.4 us
  Pallas kernels  79.4 us (100%)
    pallas_call x1, Pallas kernels, local(): pl.pallas_call(functools.partial(kernel, n_sp), out_shape=jax.ShapeDtypeS...  77.4 us
    pallas_call x1, Pallas kernels, local(): pl.pallas_call(hand_out, out_shape=jax.ShapeDtypeStruct(mixed.shape, BF16...  1.98 us

profile of v4, /device:TPU:0, one launch (start us, length us, event | category | flops | bytes accessed | tf_op | source)
XLA Modules:
  0.0 79.4 jit_solution(537331493427375199)
XLA Ops:
  0.0 77.4 %step.1.src = bf16[128,2,2048]{2,1,0:T(2,128)(2,1)} custom-call(bf16[128,2,2048]{2,1,0:T(2,128)(2,1)} %lat_hbm.1, bf16[256,2,2048]{2,1,0:T(2,128)(2,1)} %ctx_hbm.1, bf16[2,512]{1,0:T(2,128)(2,1)} %cond_ref.1, bf16[512]{0:T(512)(128)(2,1)} %cctx_ref.1, f32[1,2048]{1,0:T(1,128)} %bitcast.2, bf16[512,512]{1,0:T(8,128)(2,1)} %wsh_hbm.1, ...), custom_call_target="tpu_custom_call" | custom-call | tf_op jit(solution)/shard_map/step/pallas_call | solution.py:609
  77.4 2.0 %hand_out.1 = bf16[128,2,2048]{2,1,0:T(2,128)(2,1)} custom-call(bf16[128,2,2048]{2,1,0:T(2,128)(2,1)} %step.1.src), custom_call_target="tpu_custom_call" | custom-call | tf_op jit(solution)/shard_map/hand_out/pallas_call | solution.py:702

commit v5 on v4

--- a/solution.py
+++ b/solution.py
@@ -41,7 +41,6 @@
     row_sin,
     col_cos,
     col_sin,
-    out_hbm,
     mixed,
     lat_raw,
     lat_all,
@@ -88,7 +87,6 @@
     woc_r,
     woe_s,
     woe_r,
-    out_sem,
 ):
     rows, samples, width = lat_hbm.shape
     n_tp = mod_all.shape[0]
@@ -521,15 +519,10 @@
                         (lat_all[0, s, :, cols].astype(F32) + mod_g[s : s + 1, cols] * branch).astype(BF16)
                     )
                 mixed[:, :, cols] = jnp.swapaxes(jnp.stack(both), 0, 1)
-                out_copy(n).start()
 
     def out_cols(n):
         span = width // OUT_PIECES
         return pl.ds(pl.multiple_of(n * span, span), span)
-
-    def out_copy(n):
-        cols = out_cols(n)
-        return pltpu.make_async_copy(mixed.at[:, :, cols], out_hbm.at[:, :, cols], out_sem.at[n])
 
     hand_over(3)
     for k in range(n_tp):
@@ -562,8 +555,6 @@
             wo_core(k, p, mine_q).wait_send()
     for k in (1, 2, 3):
         wo_last(k, pair_q).wait_send()
-    for n in range(OUT_PIECES):
-        out_copy(n).wait()
 
 
 def local(
@@ -602,17 +593,16 @@
 
     row_table = table(n_sp * block // GRID_W)
     col_table = table(GRID_W)
-    hbm = pl.BlockSpec(memory_space=pl.ANY)
+    hbm = pl.BlockSpec(memory_space=pltpu.HBM)
     vmem = pl.BlockSpec(memory_space=pltpu.VMEM)
     smem = pl.BlockSpec(memory_space=pltpu.SMEM)
     dma = pltpu.SemaphoreType.DMA
     mixed = pl.pallas_call(
         functools.partial(kernel, n_sp),
-        out_shape=jax.ShapeDtypeStruct((rows, samples, width), BF16),
+        out_shape=pltpu.VMEM((rows, samples, width), BF16),
         in_specs=[hbm, hbm, vmem, vmem, vmem, hbm, hbm, hbm, hbm, hbm, hbm, hbm, smem, vmem, vmem, vmem, vmem],
-        out_specs=hbm,
+        out_specs=vmem,
         scratch_shapes=[
-            pltpu.VMEM((rows, samples, width), BF16),
             pltpu.VMEM((rows, samples, width), BF16),
             pltpu.VMEM((n_tp, samples, rows, width), BF16),
             pltpu.VMEM((lc, samples, width), BF16),
@@ -658,7 +648,6 @@
             dma((n_tp, 2)),
             dma((n_tp,)),
             dma((n_tp,)),
-            dma((OUT_PIECES,)),
         ],
         compiler_params=pltpu.CompilerParams(
             collective_id=0, has_side_effects=True, vmem_limit_bytes=60 * 1024 * 1024
@@ -681,32 +670,7 @@
         *row_table,
         *col_table,
     )
-    pieces = 4
-    piece = rows // pieces
-
-    def hand_out(src, dst, held, sems):
-        def copy(i, out):
-            part = pl.ds(i * piece, piece)
-            if out:
-                return pltpu.make_async_copy(held.at[part], dst.at[part], sems.at[1, i])
-            return pltpu.make_async_copy(src.at[part], held.at[part], sems.at[0, i])
-
-        for i in range(pieces):
-            copy(i, False).start()
-        for i in range(pieces):
-            copy(i, False).wait()
-            copy(i, True).start()
-        for i in range(pieces):
-            copy(i, True).wait()
-
-    return pl.pallas_call(
-        hand_out,
-        out_shape=jax.ShapeDtypeStruct(mixed.shape, BF16),
-        in_specs=[hbm],
-        out_specs=hbm,
-        scratch_shapes=[pltpu.VMEM((rows, samples, width), BF16), dma((2, pieces))],
-        name="hand_out",
-    )(mixed)
+    return mixed
 
 
 def solution(mesh):

time: 79.6 us -> 77.7 us (0.976)
  Pallas kernels: 79.4 us -> 76.6 us
  local copies, waits for them, and re-layouts: 0 us -> 0.97 us
    pallas_call x2 -> x1, Pallas kernels: 79.4 us -> 76.6 us  [local(): pl.pallas_call(functools.partial(kernel, n_sp), out_shape=pltpu.VMEM((row...]
    unnamed x0 -> x1, local copies, waits for them, and re-layouts: none -> 0.97 us
where the time goes in v5:
time: 77.7 us; the launch traced here: 77.6 us
  Pallas kernels  76.6 us (99%)
  local copies, waits for them, and re-layouts  0.97 us (1%)
    pallas_call x1, Pallas kernels, local(): pl.pallas_call(functools.partial(kernel, n_sp), out_shape=pltpu.VMEM((row...  76.6 us

profile of v5, /device:TPU:0, one launch (start us, length us, event | category | flops | bytes accessed | tf_op | source)
XLA Modules:
  0.0 77.6 jit_solution(3808126022125658488)
XLA Ops:
  0.0 76.6 %step.1 = bf16[128,2,2048]{2,1,0:T(2,128)(2,1)S(1)} custom-call(bf16[128,2,2048]{2,1,0:T(2,128)(2,1)} %lat_hbm.1, bf16[256,2,2048]{2,1,0:T(2,128)(2,1)} %ctx_hbm.1, bf16[2,512]{1,0:T(2,128)(2,1)} %cond_ref.1, bf16[512]{0:T(512)(128)(2,1)} %cctx_ref.1, f32[1,2048]{1,0:T(1,128)} %bitcast.2, bf16[512,512]{1,0:T(8,128)(2,1)} %wsh_hbm.1, ...), custom_call_target="tpu_custom_call" | custom-call | tf_op jit(solution)/shard_map/step/pallas_call | solution.py:600
  76.6 1.0 %copy.19 = bf16[128,2,2048]{2,1,0:T(2,128)(2,1)} copy(bf16[128,2,2048]{2,1,0:T(2,128)(2,1)S(1)} %step.1) | data formatting | bytes 2097152

commit v6 on v5

--- a/solution.py
+++ b/solution.py
@@ -142,7 +142,7 @@
     def direct(k, s, p):
         part = pl.ds(p * half, half)
         return remote(
-            lat_all.at[0, s, part], lat_all.at[k, s, part], lat_s.at[k, s, p], lat_r.at[k, s, p], {"tp": peer[k]}
+            lat_all.at[0, s, part], lat_all.at[k, s, part], lat_s.at[k - 1, s, p], lat_r.at[k - 1, s, p], {"tp": peer[k]}
         )
 
     def relay(s, p):
@@ -164,7 +164,7 @@
 
     def wo_direct(k, p):
         part = wo_half(mine_q, p)
-        return remote(wo_all.at[0, part], wo_all.at[k, part], wo_s.at[k, p], wo_r.at[k, p], {"tp": peer[k]})
+        return remote(wo_all.at[0, part], wo_all.at[k, part], wo_s.at[k - 1, p], wo_r.at[k - 1, p], {"tp": peer[k]})
 
     def wo_relay(p):
         part = wo_half(mine_q, p)
@@ -173,12 +173,12 @@
         )
 
     def wo_pair(k, p, index):
-        part = wo_all.at[k, wo_half(index, p)]
-        return remote(part, part, woz_s.at[k, p], woz_r.at[k, p], {"sp": sp + 1 - 2 * zh})
+        part = wo_all.at[k, wo_rows(index) if p is None else wo_half(index, p)]
+        return remote(part, part, woz_s.at[k - 1], woz_r.at[k - 1], {"sp": sp + 1 - 2 * zh})
 
     def wo_core(k, p, index):
-        part = wo_all.at[k, wo_half(index, p)]
-        return remote(part, part, woc_s.at[k, p], woc_r.at[k, p], {"dp": 1 - dp})
+        part = wo_all.at[k, wo_rows(index) if p is None else wo_half(index, p)]
+        return remote(part, part, woc_s.at[k - 1], woc_r.at[k - 1], {"dp": 1 - dp})
 
     def wo_share(k, p):
         wo_pair(k, p, mine_q).start()
@@ -186,7 +186,7 @@
 
     def wo_last(k, index):
         part = wo_all.at[k, wo_rows(index)]
-        return remote(part, part, woe_s.at[k], woe_r.at[k], {"dp": 1 - dp})
+        return remote(part, part, woe_s.at[k - 1], woe_r.at[k - 1], {"dp": 1 - dp})
 
     loads[8].wait()
     wo_direct(1, 0).start()
@@ -202,7 +202,7 @@
         loads[m].wait()
         mod_p[0, :, m * wid : (m + 1) * wid] = jnp.dot(both, wmod[m], preferred_element_type=F32)[0:4]
     mod_copies = [
-        remote(mod_p.at[0], mod_p.at[o], modp_s.at[o], modp_r.at[o], {"sp": sp_peer(o)})
+        remote(mod_p.at[0], mod_p.at[o], modp_s.at[o - 1], modp_r.at[o - 1], {"sp": sp_peer(o)})
         for o in range(1, n_sp)
     ]
     for copy in mod_copies:
@@ -232,7 +232,7 @@
         total = total + mod_p[o]
     mod_all[tp] = total
     all_copies = [
-        remote(mod_all.at[tp], mod_all.at[tp], moda_s.at[k], moda_r.at[k], {"tp": peer[k]})
+        remote(mod_all.at[tp], mod_all.at[tp], moda_s.at[k - 1], moda_r.at[k - 1], {"tp": peer[k]})
         for k in (1, 2, 3)
     ]
     for copy in all_copies:
@@ -249,7 +249,7 @@
     wo_share(2, 1)
     for k in (1, 2, 3):
         remote(
-            mod_all.at[peer[k]], mod_all.at[peer[k]], moda_s.at[k], moda_r.at[k], {"tp": peer[k]}
+            mod_all.at[peer[k]], mod_all.at[peer[k]], moda_s.at[k - 1], moda_r.at[k - 1], {"tp": peer[k]}
         ).wait_recv()
     for t in range(n_tp):
         cols = slice(t * wid, (t + 1) * wid)
@@ -286,7 +286,7 @@
 
     mine = ckv.at[:, pl.ds(ctx_at, lc), :]
     ctx_copies = [
-        remote(mine, mine, ctx_s.at[o], ctx_r.at[o], {"sp": sp_peer(o)}) for o in range(1, n_sp)
+        remote(mine, mine, ctx_s.at[o - 1], ctx_r.at[o - 1], {"sp": sp_peer(o)}) for o in range(1, n_sp)
     ]
     for copy in ctx_copies:
         copy.start()
@@ -342,10 +342,8 @@
     def _():
         kvbuf[:, WINDOW + block :, :] = jnp.zeros((samples, WINDOW, 2 * kw), BF16)
 
-    acc[...] = jnp.zeros_like(acc)
-
     def attn_copy(k, s, dest):
-        return remote(attn.at[n_tp + k, s], attn.at[k, s], attn_s.at[k, s], attn_r.at[k, s], {"tp": dest})
+        return remote(attn.at[n_tp + k, s], attn.at[k, s], attn_s.at[k - 1, s], attn_r.at[k - 1, s], {"tp": dest})
 
     def project(blocks):
         spots = []
@@ -396,9 +394,45 @@
     row_id = lax.broadcasted_iota(jnp.int32, (pair, 1), 0)
 
     def hand_over(k):
+        wo_pair(k, None, pair_q).wait_recv()
+        wo_last(k, pair_q).start()
+
+    def out_cols(n):
+        span = width // OUT_PIECES
+        return pl.ds(pl.multiple_of(n * span, span), span)
+
+    def project_own(s):
+        held = pl.ds(s * rows, rows)
+
+        @pl.loop(0, OUT_PIECES)
+        def _(n):
+            cols = out_cols(n)
+            part = jnp.dot(attn[0, s], wo_all[0, :, cols], preferred_element_type=F32)
+            acc[held, cols] = part.astype(BF16).astype(F32)
+
+    def edges_sent(s):
+        @pl.when(not_last)
+        def _():
+            halo_up(s).wait_send()
+
+        @pl.when(not_first)
+        def _():
+            halo_down(s).wait_send()
+
+    def early_sent():
+        for copy in mod_copies + all_copies + ctx_copies:
+            copy.wait_send()
         for p in range(2):
-            wo_pair(k, p, pair_q).wait_recv()
-        wo_last(k, pair_q).start()
+            for k in (1, 2):
+                for s in range(samples):
+                    direct(k, s, p).wait_send()
+                wo_direct(k, p).wait_send()
+            relay(0, p).wait_send()
+            wo_relay(p).wait_send()
+        for k in (1, 2):
+            wo_pair(k, None, mine_q).wait_send()
+            wo_core(k, None, mine_q).wait_send()
+        edges_sent(0)
 
     def attend(i, s):
         k = jnp.where(i == 0, 1, jnp.where(i < n_tp - 1, n_tp - i, 0))
@@ -461,6 +495,11 @@
         def _(i):
             @pl.when(i == s)
             def _():
+                @pl.when(s == 1)
+                def _():
+                    project_own(0)
+                    early_sent()
+
                 relay(s, 0).wait_recv()
                 relay(s, 1).wait_recv()
                 project([(3, s)])
@@ -472,7 +511,7 @@
                     wo_share(2, 0)
                     for o in range(1, n_sp):
                         got = ckv.at[:, pl.ds(pl.multiple_of(sp_peer(n_sp - o) * lc, lc), lc), :]
-                        remote(got, got, ctx_s.at[o], ctx_r.at[o], {"sp": sp_peer(o)}).wait_recv()
+                        remote(got, got, ctx_s.at[o - 1], ctx_r.at[o - 1], {"sp": sp_peer(o)}).wait_recv()
                     wo_relay(0).wait_recv()
                     wo_share(3, 0)
 
@@ -494,67 +533,52 @@
             for k in (3, 2, 1):
                 attn_copy(k, 0, peer[k]).start()
 
-    def project_out(k):
+    def arrived(k, s):
         if k > 0:
-            for p in range(2):
-                wo_core(k, p, mine_q + 1 - 2 * dp).wait_recv()
-            wo_last(k, pair_q + 1 - 2 * dp).wait_recv()
-            for s in range(samples):
-                attn_copy(k, s, peer[k]).wait_recv()
+            if s == 0:
+                wo_core(k, None, mine_q + 1 - 2 * dp).wait_recv()
+                wo_last(k, pair_q + 1 - 2 * dp).wait_recv()
+            attn_copy(k, s, peer[k]).wait_recv()
+
+    def project_out(k, s, last):
+        arrived(k, s)
 
         @pl.loop(0, OUT_PIECES)
         def _(n):
             cols = out_cols(n)
-            part = jnp.dot(
-                attn[k].reshape(samples * rows, qw), wo_all[k, :, cols], preferred_element_type=F32
-            )
-            total = acc[:, cols] + part.astype(BF16).astype(F32)
-            if k < n_tp - 1:
-                acc[:, cols] = total
+            part = jnp.dot(attn[k, s], wo_all[k, :, cols], preferred_element_type=F32)
+            held = pl.ds(s * rows, rows)
+            total = acc[held, cols] + part.astype(BF16).astype(F32)
+            if not last:
+                acc[held, cols] = total
             else:
                 both = []
-                for s in range(samples):
-                    branch = total[s * rows : (s + 1) * rows]
+                for t in range(samples):
+                    branch = total if t == s else acc[t * rows : (t + 1) * rows, cols]
                     both.append(
-                        (lat_all[0, s, :, cols].astype(F32) + mod_g[s : s + 1, cols] * branch).astype(BF16)
+                        (lat_all[0, t, :, cols].astype(F32) + mod_g[t : t + 1, cols] * branch).astype(BF16)
                     )
                 mixed[:, :, cols] = jnp.swapaxes(jnp.stack(both), 0, 1)
 
-    def out_cols(n):
-        span = width // OUT_PIECES
-        return pl.ds(pl.multiple_of(n * span, span), span)
-
     hand_over(3)
-    for k in range(n_tp):
-        project_out(k)
-
-    for copy in mod_copies + all_copies + ctx_copies:
-        copy.wait_send()
+    project_own(1)
+    project_out(1, 0, False)
+    project_out(2, 0, False)
+    project_out(3, 0, False)
+    project_out(3, 1, False)
+    project_out(1, 1, False)
+    project_out(2, 1, True)
+
     for s in range(samples):
-        for p in range(2):
-            direct(1, s, p).wait_send()
-            direct(2, s, p).wait_send()
-            relay(s, p).wait_send()
         for k in (1, 2, 3):
             attn_copy(k, s, peer[k]).wait_send()
-
-        @pl.when(not_last)
-        def _(s=s):
-            halo_up(s).wait_send()
-
-        @pl.when(not_first)
-        def _(s=s):
-            halo_down(s).wait_send()
-
     for p in range(2):
-        wo_direct(1, p).wait_send()
-        wo_direct(2, p).wait_send()
-        wo_relay(p).wait_send()
-        for k in (1, 2, 3):
-            wo_pair(k, p, mine_q).wait_send()
-            wo_core(k, p, mine_q).wait_send()
+        relay(1, p).wait_send()
     for k in (1, 2, 3):
         wo_last(k, pair_q).wait_send()
+    wo_pair(3, None, mine_q).wait_send()
+    wo_core(3, None, mine_q).wait_send()
+    edges_sent(1)
 
 
 def local(
@@ -624,30 +648,30 @@
             pltpu.VMEM((block, HEAD_DIM), F32),
             pltpu.VMEM((block, HEAD_DIM), F32),
             dma((9,)),
-            dma((n_sp,)),
-            dma((n_sp,)),
-            dma((n_tp,)),
-            dma((n_tp,)),
-            dma((n_tp, samples, 2)),
-            dma((n_tp, samples, 2)),
+            dma((n_sp - 1,)),
+            dma((n_sp - 1,)),
+            dma((n_tp - 1,)),
+            dma((n_tp - 1,)),
+            dma((2, samples, 2)),
+            dma((2, samples, 2)),
             dma((samples, 2)),
             dma((samples, 2)),
-            dma((n_sp,)),
-            dma((n_sp,)),
+            dma((n_sp - 1,)),
+            dma((n_sp - 1,)),
             dma((2, samples)),
             dma((2, samples)),
-            dma((n_tp, samples)),
-            dma((n_tp, samples)),
-            dma((n_tp, 2)),
-            dma((n_tp, 2)),
+            dma((n_tp - 1, samples)),
+            dma((n_tp - 1, samples)),
+            dma((2, 2)),
+            dma((2, 2)),
             dma((2,)),
             dma((2,)),
-            dma((n_tp, 2)),
-            dma((n_tp, 2)),
-            dma((n_tp, 2)),
-            dma((n_tp, 2)),
-            dma((n_tp,)),
-            dma((n_tp,)),
+            dma((n_tp - 1,)),
+            dma((n_tp - 1,)),
+            dma((n_tp - 1,)),
+            dma((n_tp - 1,)),
+            dma((n_tp - 1,)),
+            dma((n_tp - 1,)),
         ],
         compiler_params=pltpu.CompilerParams(
             collective_id=0, has_side_effects=True, vmem_limit_bytes=60 * 1024 * 1024

time: 77.7 us -> 76.9 us (0.990); the launches traced: 77.6 us -> 76 us
  Pallas kernels: 76.6 us -> 75 us
    pallas_call x1, Pallas kernels: 76.6 us -> 75 us  [local(): pl.pallas_call(functools.partial(kernel, n_sp), out_shape=pltpu.VMEM((row...]
where the time goes in v6:
time: 76.9 us; the launch traced here: 76 us
  Pallas kernels  75 us (98%)
  local copies, waits for them, and re-layouts  0.97 us (1%)
    pallas_call x1, Pallas kernels, local(): pl.pallas_call(functools.partial(kernel, n_sp), out_shape=pltpu.VMEM((row...  75 us

profile of v6, /device:TPU:0, one launch (start us, length us, event | category | flops | bytes accessed | tf_op | source)
XLA Modules:
  0.0 76.0 jit_solution(9913229789169595680)
XLA Ops:
  0.0 75.0 %step.1 = bf16[128,2,2048]{2,1,0:T(2,128)(2,1)S(1)} custom-call(bf16[128,2,2048]{2,1,0:T(2,128)(2,1)} %lat_hbm.1, bf16[256,2,2048]{2,1,0:T(2,128)(2,1)} %ctx_hbm.1, bf16[2,512]{1,0:T(2,128)(2,1)} %cond_ref.1, bf16[512]{0:T(512)(128)(2,1)} %cctx_ref.1, f32[1,2048]{1,0:T(1,128)} %bitcast.2, bf16[512,512]{1,0:T(8,128)(2,1)} %wsh_hbm.1, ...), custom_call_target="tpu_custom_call" | custom-call | tf_op jit(solution)/shard_map/step/pallas_call | solution.py:624
  75.0 1.0 %copy.19 = bf16[128,2,2048]{2,1,0:T(2,128)(2,1)} copy(bf16[128,2,2048]{2,1,0:T(2,128)(2,1)S(1)} %step.1) | data formatting | bytes 2097152

commit v7 on v6

--- a/solution.py
+++ b/solution.py
@@ -491,6 +491,11 @@
         project([(1, s), (2, s)])
         send_edges(s, inner, inner)
 
+        @pl.when((s == 1) & inner & (dp == 0))
+        def _():
+            wo_relay(1).wait_recv()
+            wo_share(3, 1)
+
         @pl.loop(0, n_tp)
         def _(i):
             @pl.when(i == s)
@@ -517,8 +522,11 @@
 
                 @pl.when(s == 1)
                 def _():
-                    wo_relay(1).wait_recv()
-                    wo_share(3, 1)
+                    @pl.when(at_first | at_last | (dp == 1))
+                    def _():
+                        wo_relay(1).wait_recv()
+                        wo_share(3, 1)
+
                     hand_over(1)
                     hand_over(2)
 
@@ -564,10 +572,12 @@
     project_own(1)
     project_out(1, 0, False)
     project_out(2, 0, False)
-    project_out(3, 0, False)
-    project_out(3, 1, False)
-    project_out(1, 1, False)
-    project_out(2, 1, True)
+    for core, order in enumerate((((3, 0), (3, 1), (1, 1), (2, 1)), ((1, 1), (2, 1), (3, 0), (3, 1)))):
+
+        @pl.when(dp == core)
+        def _(order=order):
+            for k, s in order:
+                project_out(k, s, (k, s) == order[-1])
 
     for s in range(samples):
         for k in (1, 2, 3):

time: 76.9 us -> 76.1 us (0.990); the launches traced: 76 us -> 76 us
  no operation moved by 1% of the time
where the time goes in v7:
time: 76.1 us; the launch traced here: 76 us
  Pallas kernels  75 us (99%)
  local copies, waits for them, and re-layouts  0.97 us (1%)
    pallas_call x1, Pallas kernels, local(): pl.pallas_call(functools.partial(kernel, n_sp), out_shape=pltpu.VMEM((row...  75 us

profile of v7, /device:TPU:0, one launch (start us, length us, event | category | flops | bytes accessed | tf_op | source)
XLA Modules:
  0.0 76.0 jit_solution(2230934784686386989)
XLA Ops:
  0.0 75.0 %step.1 = bf16[128,2,2048]{2,1,0:T(2,128)(2,1)S(1)} custom-call(bf16[128,2,2048]{2,1,0:T(2,128)(2,1)} %lat_hbm.1, bf16[256,2,2048]{2,1,0:T(2,128)(2,1)} %ctx_hbm.1, bf16[2,512]{1,0:T(2,128)(2,1)} %cond_ref.1, bf16[512]{0:T(512)(128)(2,1)} %cctx_ref.1, f32[1,2048]{1,0:T(1,128)} %bitcast.2, bf16[512,512]{1,0:T(8,128)(2,1)} %wsh_hbm.1, ...), custom_call_target="tpu_custom_call" | custom-call | tf_op jit(solution)/shard_map/step/pallas_call | solution.py:634
  75.0 1.0 %copy.19 = bf16[128,2,2048]{2,1,0:T(2,128)(2,1)} copy(bf16[128,2,2048]{2,1,0:T(2,128)(2,1)S(1)} %step.1) | data formatting | bytes 2097152

commit v8 on v7

--- a/solution.py
+++ b/solution.py
@@ -19,7 +19,7 @@
 BF16 = jnp.bfloat16
 LOG2E = math.log2(math.e)
 CHUNK = 16
-OUT_PIECES = 2
+OUT_PIECES = 1
 
 
 def kernel(
@@ -530,6 +530,10 @@
                     hand_over(1)
                     hand_over(2)
 
+            @pl.when((s == 1) & (i == n_tp - 1) & (dp == 1))
+            def _():
+                hand_over(3)
+
             attend(i, s)
 
         @pl.when(s == 0)
@@ -568,7 +572,10 @@
                     )
                 mixed[:, :, cols] = jnp.swapaxes(jnp.stack(both), 0, 1)
 
-    hand_over(3)
+    @pl.when(dp == 0)
+    def _():
+        hand_over(3)
+
     project_own(1)
     project_out(1, 0, False)
     project_out(2, 0, False)

time: 76.1 us -> 76 us (level)
  no operation moved by 1% of the time
where the time goes in v8:
time: 76 us; the launch traced here: 75.8 us
  Pallas kernels  74.8 us (98%)
  local copies, waits for them, and re-layouts  0.97 us (1%)
    pallas_call x1, Pallas kernels, local(): pl.pallas_call(functools.partial(kernel, n_sp), out_shape=pltpu.VMEM((row...  74.8 us

profile of v8, /device:TPU:0, one launch (start us, length us, event | category | flops | bytes accessed | tf_op | source)
XLA Modules:
  0.0 75.8 jit_solution(4931856023416770394)
XLA Ops:
  0.0 74.8 %step.1 = bf16[128,2,2048]{2,1,0:T(2,128)(2,1)S(1)} custom-call(bf16[128,2,2048]{2,1,0:T(2,128)(2,1)} %lat_hbm.1, bf16[256,2,2048]{2,1,0:T(2,128)(2,1)} %ctx_hbm.1, bf16[2,512]{1,0:T(2,128)(2,1)} %cond_ref.1, bf16[512]{0:T(512)(128)(2,1)} %cctx_ref.1, f32[1,2048]{1,0:T(1,128)} %bitcast.2, bf16[512,512]{1,0:T(8,128)(2,1)} %wsh_hbm.1, ...), custom_call_target="tpu_custom_call" | custom-call | tf_op jit(solution)/shard_map/step/pallas_call | solution.py:641
  74.8 1.0 %copy.19 = bf16[128,2,2048]{2,1,0:T(2,128)(2,1)} copy(bf16[128,2,2048]{2,1,0:T(2,128)(2,1)S(1)} %step.1) | data formatting | bytes 2097152

commit v9 on v8

--- a/solution.py
+++ b/solution.py
@@ -142,7 +142,7 @@
     def direct(k, s, p):
         part = pl.ds(p * half, half)
         return remote(
-            lat_all.at[0, s, part], lat_all.at[k, s, part], lat_s.at[k - 1, s, p], lat_r.at[k - 1, s, p], {"tp": peer[k]}
+            lat_all.at[0, s, part], lat_all.at[k, s, part], lat_s.at[k - 1], lat_r.at[k - 1, s, p], {"tp": peer[k]}
         )
 
     def relay(s, p):
@@ -164,7 +164,7 @@
 
     def wo_direct(k, p):
         part = wo_half(mine_q, p)
-        return remote(wo_all.at[0, part], wo_all.at[k, part], wo_s.at[k - 1, p], wo_r.at[k - 1, p], {"tp": peer[k]})
+        return remote(wo_all.at[0, part], wo_all.at[k, part], wo_s.at[k - 1], wo_r.at[k - 1, p], {"tp": peer[k]})
 
     def wo_relay(p):
         part = wo_half(mine_q, p)
@@ -343,7 +343,7 @@
         kvbuf[:, WINDOW + block :, :] = jnp.zeros((samples, WINDOW, 2 * kw), BF16)
 
     def attn_copy(k, s, dest):
-        return remote(attn.at[n_tp + k, s], attn.at[k, s], attn_s.at[k - 1, s], attn_r.at[k - 1, s], {"tp": dest})
+        return remote(attn.at[n_tp + k, s], attn.at[k, s], attn_s.at[k - 1], attn_r.at[k - 1, s], {"tp": dest})
 
     def project(blocks):
         spots = []
@@ -423,13 +423,16 @@
         for copy in mod_copies + all_copies + ctx_copies:
             copy.wait_send()
         for p in range(2):
-            for k in (1, 2):
-                for s in range(samples):
-                    direct(k, s, p).wait_send()
-                wo_direct(k, p).wait_send()
             relay(0, p).wait_send()
             wo_relay(p).wait_send()
         for k in (1, 2):
+            remote(
+                lat_all.at[0], lat_all.at[k], lat_s.at[k - 1], lat_r.at[k - 1, 0, 0], {"tp": peer[k]}
+            ).wait_send()
+            part = wo_rows(mine_q)
+            remote(
+                wo_all.at[0, part], wo_all.at[k, part], wo_s.at[k - 1], wo_r.at[k - 1, 0], {"tp": peer[k]}
+            ).wait_send()
             wo_pair(k, None, mine_q).wait_send()
             wo_core(k, None, mine_q).wait_send()
         edges_sent(0)
@@ -586,9 +589,10 @@
             for k, s in order:
                 project_out(k, s, (k, s) == order[-1])
 
-    for s in range(samples):
-        for k in (1, 2, 3):
-            attn_copy(k, s, peer[k]).wait_send()
+    for k in (1, 2, 3):
+        remote(
+            attn.at[n_tp + k], attn.at[k], attn_s.at[k - 1], attn_r.at[k - 1, 0], {"tp": peer[k]}
+        ).wait_send()
     for p in range(2):
         relay(1, p).wait_send()
     for k in (1, 2, 3):
@@ -669,7 +673,7 @@
             dma((n_sp - 1,)),
             dma((n_tp - 1,)),
             dma((n_tp - 1,)),
-            dma((2, samples, 2)),
+            dma((2,)),
             dma((2, samples, 2)),
             dma((samples, 2)),
             dma((samples, 2)),
@@ -677,9 +681,9 @@
             dma((n_sp - 1,)),
             dma((2, samples)),
             dma((2, samples)),
+            dma((n_tp - 1,)),
             dma((n_tp - 1, samples)),
-            dma((n_tp - 1, samples)),
-            dma((2, 2)),
+            dma((2,)),
             dma((2, 2)),
             dma((2,)),
             dma((2,)),

time: 76 us -> 75.9 us (level)
  no operation moved by 1% of the time
where the time goes in v9:
time: 75.9 us; the launch traced here: 75.7 us
  Pallas kernels  74.7 us (98%)
  local copies, waits for them, and re-layouts  0.97 us (1%)
    pallas_call x1, Pallas kernels, local(): pl.pallas_call(functools.partial(kernel, n_sp), out_shape=pltpu.VMEM((row...  74.7 us

profile of v9, /device:TPU:0, one launch (start us, length us, event | category | flops | bytes accessed | tf_op | source)
XLA Modules:
  0.0 75.7 jit_solution(1975645932686891919)
XLA Ops:
  0.0 74.7 %step.1 = bf16[128,2,2048]{2,1,0:T(2,128)(2,1)S(1)} custom-call(bf16[128,2,2048]{2,1,0:T(2,128)(2,1)} %lat_hbm.1, bf16[256,2,2048]{2,1,0:T(2,128)(2,1)} %ctx_hbm.1, bf16[2,512]{1,0:T(2,128)(2,1)} %cond_ref.1, bf16[512]{0:T(512)(128)(2,1)} %cctx_ref.1, f32[1,2048]{1,0:T(1,128)} %bitcast.2, bf16[512,512]{1,0:T(8,128)(2,1)} %wsh_hbm.1, ...), custom_call_target="tpu_custom_call" | custom-call | tf_op jit(solution)/shard_map/step/pallas_call | solution.py:645
  74.7 1.0 %copy.19 = bf16[128,2,2048]{2,1,0:T(2,128)(2,1)} copy(bf16[128,2,2048]{2,1,0:T(2,128)(2,1)S(1)} %step.1) | data formatting | bytes 2097152
